TPU v7x, 256 devices: a whole 4x4x8 slice. The times are simulated.
256 devices in a mesh: ep: 64 (over z, x, core), tp: 4 (over y).
Axes of the slice: x: 4, y: 4, z: 8, core: 2. Of those that a mesh axis runs over, the one named last changes fastest.
Arguments:
- mixer_input: bfloat16 [32768, 2048], P('ep'), may hold values from -5.5 to 5.5
- expert_input: bfloat16 [32768, 2048], P('ep'), may hold values from -6 to 6
- gain_mixer: float32 [2048], replicated, may hold values from 0.1 to 1.9
- gain_expert: float32 [2048], replicated, may hold values from 0.1 to 1.9
- query_weight: bfloat16 [2048, 1536], P(None, 'tp')
- key_weight: bfloat16 [2048, 256], P(None, 'tp')
- value_weight: bfloat16 [2048, 256], P(None, 'tp'), may hold values from -0.125 to 0.125
- sink_logits: float32 [24], P('tp'), may hold values from 2 to 6
- output_weight: bfloat16 [1536, 2048], P('tp'), may hold values from -0.75 to 0.75
- expert_choice: int32 [32768, 2], P('ep'), may hold values from 0 to 63, all different within a row; in each aligned block of 128 rows (0 to 127, 128 to 255, ...) at most 8 rows name the same one
- route_weights: float32 [32768, 2], P('ep'), may hold values from 0.2 to 1.2
- expert_gate: bfloat16 [64, 2048, 1024], P('ep', None, 'tp'), may hold values from -0.125 to 0.125
- expert_up: bfloat16 [64, 2048, 1024], P('ep', None, 'tp'), may hold values from -0.125 to 0.125
- expert_down: bfloat16 [64, 1024, 2048], P('ep', 'tp'), may hold values from -0.1875 to 0.1875
- shared_gate: bfloat16 [2048, 512], P(None, 'tp'), may hold values from -0.125 to 0.125
- shared_up: bfloat16 [2048, 512], P(None, 'tp'), may hold values from -0.125 to 0.125
- shared_down: bfloat16 [512, 2048], P('tp'), may hold values from -0.25 to 0.25
Outputs:
- mixer_output: bfloat16 [32768, 2048], P(('ep', 'tp'))
- expert_output: bfloat16 [32768, 2048], P(('ep', 'tp'))
Inputs may be any that keep to these rules, and one draw needn't show every extreme that they name: `expert_choice`: in each aligned block of 128 rows no expert is named by more than 8 rows, and in some block some expert is named by exactly 8 rows; the 2 entries of a row differ.
All inputs are finite; a program needn't handle non-finite values.
Results may differ from a plain program's by a relative error of at most 0.019.
Values may be sent and summed in bfloat16 or wider, within the bound.
A program may use at most 128 MiB of HBM per device.

v0:
```python
import math

import jax
import jax.numpy as jnp
from jax import lax
from jax.sharding import PartitionSpec as P

HEAD_DIM = 64
WINDOW = 128
SEQS = 1


norm_eps = 1e-06
rope_base = 500000.0


def from_behind(value, axis, steps):
    count = lax.axis_size(axis)
    first, last = (max(0, -steps), min(count, count - steps))
    return lax.ppermute(value, axis, [(source, source + steps) for source in range(first, last)])


def cut_along(shard, dim, count):
    lengths = shard.shape
    pieces = shard.reshape(*lengths[:dim], count, lengths[dim] // count, *lengths[dim + 1 :])
    return jnp.moveaxis(pieces, dim, 0)


def sent_and_summed(shard, axis, dim):
    pieces = cut_along(shard, dim, lax.axis_size(axis))
    arrived = lax.all_to_all(pieces, axis, split_axis=0, concat_axis=0, tiled=True)
    return arrived.astype(jnp.float32).sum(axis=0)


def rounded(value):
    return lax.optimization_barrier(value.astype(jnp.bfloat16)).astype(jnp.float32)


def rms_scale(matrix, scaling):
    widened = matrix.astype(jnp.float32)
    scaled = widened * lax.rsqrt(jnp.mean(widened * widened, axis=-1, keepdims=True) + norm_eps)
    return (scaled * scaling).astype(jnp.bfloat16)


def frequencies(head_size):
    half_steps = jnp.arange(head_size // 2, dtype=jnp.float32)
    return rope_base ** (-(2.0 * half_steps) / head_size)


def rotate(heads, angles):
    middle = heads.shape[-1] // 2
    widened = heads.astype(jnp.float32)
    cosine = jnp.cos(angles)[:, None, :]
    sine_val = jnp.sin(angles)[:, None, :]
    leading = widened[..., :middle]
    trailing = widened[..., middle:]
    turned = jnp.concatenate(
        [leading * cosine - trailing * sine_val, trailing * cosine + leading * sine_val], axis=-1
    )
    return turned.astype(jnp.bfloat16)


def attend(
    query_heads, key_heads, value_heads, prior_keys, prior_values, first_position, sink_logits
):
    window = prior_keys.shape[0]
    total_rows, kv_count, head_size = key_heads.shape
    group_size = query_heads.shape[1] // kv_count
    blocks = total_rows // window

    def banded(earlier, current):
        joined = jnp.concatenate([earlier, current], axis=0).reshape(
            blocks + 1, window, kv_count, head_size
        )
        return jnp.concatenate([joined[:-1], joined[1:]], axis=1)

    band_keys = banded(prior_keys, key_heads)
    band_values = banded(prior_values, value_heads)
    query_blocks = query_heads.reshape(blocks, window, kv_count, group_size, head_size)
    scores = jnp.einsum(
        "nqhgd,nkhd->nhgqk", query_blocks, band_keys, preferred_element_type=jnp.float32
    ) / math.sqrt(head_size)
    query_index = jnp.arange(window, dtype=jnp.int32)[:, None]
    key_index = jnp.arange(2 * window, dtype=jnp.int32)[None, :]
    distance = query_index + window - key_index
    block_start = first_position + jnp.arange(blocks, dtype=jnp.int32)[:, None, None] * window
    allowed = (distance >= 0) & (distance < window) & (block_start - window + key_index >= 0)
    scores = jnp.where(allowed[:, None, None, :, :], scores, -jnp.inf)
    sink_grid = sink_logits.reshape(kv_count, group_size)[None, :, :, None, None]
    row_peak = jnp.maximum(jnp.max(scores, axis=-1, keepdims=True), sink_grid)
    shifted_exp = jnp.exp(scores - row_peak)
    denominator = jnp.sum(shifted_exp, axis=-1, keepdims=True) + jnp.exp(sink_grid - row_peak)
    probs = (shifted_exp / denominator).astype(jnp.bfloat16)
    attended = jnp.einsum(
        "nhgqk,nkhd->nqhgd", probs, band_values, preferred_element_type=jnp.float32
    )
    return attended.astype(jnp.bfloat16).reshape(total_rows, kv_count * group_size * head_size)


def local(
    mixer_input,
    expert_input,
    gain_mixer,
    gain_expert,
    query_weight,
    key_weight,
    value_weight,
    sink_logits,
    output_weight,
    expert_choice,
    route_weights,
    expert_gate,
    expert_up,
    expert_down,
    shared_gate,
    shared_up,
    shared_down,
):
    tp_count = lax.axis_size("tp")
    ep_count = lax.axis_size("ep")
    tp_rank = lax.axis_index("tp")
    group_rows, model_width = mixer_input.shape
    normed = rms_scale(mixer_input, gain_mixer)
    queries = jnp.dot(normed, query_weight, preferred_element_type=jnp.float32).astype(jnp.bfloat16)
    key_rows = jnp.dot(normed, key_weight, preferred_element_type=jnp.float32).astype(jnp.bfloat16)
    value_rows = jnp.dot(normed, value_weight, preferred_element_type=jnp.float32).astype(
        jnp.bfloat16
    )
    first_position = lax.axis_index("ep") % (ep_count // SEQS) * group_rows
    positions = (first_position + jnp.arange(group_rows, dtype=jnp.int32)).astype(jnp.float32)
    angles = positions[:, None] * frequencies(HEAD_DIM)[None, :]
    rot_queries = rotate(queries.reshape(group_rows, -1, HEAD_DIM), angles)
    rot_keys = rotate(key_rows.reshape(group_rows, -1, HEAD_DIM), angles)
    key_width = key_rows.shape[1]
    tail_start = group_rows - WINDOW
    tail_pair = jnp.concatenate(
        [rot_keys.reshape(group_rows, key_width)[tail_start:], value_rows[tail_start:]], axis=1
    )
    earlier_pair = from_behind(tail_pair, "ep", 1)
    prior_keys = earlier_pair[:, :key_width].reshape(WINDOW, -1, HEAD_DIM)
    prior_values = earlier_pair[:, key_width:].reshape(WINDOW, -1, HEAD_DIM)
    attended = attend(
        rot_queries,
        rot_keys,
        value_rows.reshape(group_rows, -1, HEAD_DIM),
        prior_keys,
        prior_values,
        first_position,
        sink_logits,
    )
    picked = attended
    mixer_output = lax.psum_scatter(
        rounded(jnp.dot(picked, output_weight, preferred_element_type=jnp.float32)).astype(
            jnp.bfloat16
        ),
        "tp",
        scatter_dimension=0,
        tiled=True,
    )
    normed_rows = rms_scale(expert_input, gain_expert)
    group_tokens = normed_rows.shape[0]
    own_tokens = group_tokens // tp_count
    top_count = expert_choice.shape[1]
    local_experts = expert_gate.shape[0]
    experts_all = local_experts * ep_count
    capacity = 2 * own_tokens * top_count // experts_all
    assigned = own_tokens * top_count
    picked_experts = expert_choice.reshape(tp_count, assigned)
    onehot = (
        picked_experts[:, :, None] == jnp.arange(experts_all, dtype=jnp.int32)[None, None, :]
    ).astype(jnp.int32)
    slot_ranks = jnp.sum(jnp.cumsum(onehot, axis=1) * onehot, axis=-1) - 1
    padded_rows = jnp.concatenate([normed_rows, jnp.zeros((1, model_width), jnp.bfloat16)], axis=0)

    def own_slot_index():
        own_experts = lax.dynamic_index_in_dim(picked_experts, tp_rank, 0, keepdims=False)
        own_ranks = lax.dynamic_index_in_dim(slot_ranks, tp_rank, 0, keepdims=False)
        return own_experts * capacity + own_ranks

    own_owner = tp_rank * own_tokens + jnp.arange(assigned, dtype=jnp.int32) // top_count
    slot_table = (
        jnp.full((experts_all * capacity,), group_tokens, jnp.int32)
        .at[own_slot_index()]
        .set(own_owner)
    )
    outgoing = padded_rows[slot_table].reshape(experts_all, 1, capacity, model_width)
    arrived = lax.all_gather(
        lax.all_to_all(outgoing, "ep", split_axis=0, concat_axis=0, tiled=True),
        "tp",
        axis=1,
        tiled=True,
    )
    sources = arrived.shape[0] // local_experts
    shaped = arrived.reshape(
        sources, local_experts, arrived.shape[1], arrived.shape[2], arrived.shape[3]
    )
    gate_values = jnp.einsum(
        "iejcd,edf->iejcf", shaped, expert_gate, preferred_element_type=jnp.float32
    )
    up_values = jnp.einsum(
        "iejcd,edf->iejcf", shaped, expert_up, preferred_element_type=jnp.float32
    )
    hidden = (jax.nn.silu(gate_values) * up_values).astype(jnp.bfloat16)
    result = jnp.einsum("iejcf,efd->iejcd", hidden, expert_down, preferred_element_type=jnp.float32)
    partials = result.astype(jnp.bfloat16).reshape(arrived.shape)
    summed = sent_and_summed(partials.astype(jnp.float32).astype(jnp.bfloat16), "tp", 1)
    returned = (
        lax.all_to_all(summed.astype(jnp.bfloat16), "ep", split_axis=0, concat_axis=0, tiled=True)
        .astype(summed.dtype)
        .reshape(-1, model_width)
    )
    own_weights = lax.dynamic_slice_in_dim(route_weights, tp_rank * own_tokens, own_tokens, 0)
    gathered = returned[own_slot_index().reshape(own_tokens, top_count)]
    routed = jnp.sum(gathered * own_weights[:, :, None], axis=1)
    picked = normed_rows
    gate_values = jnp.dot(picked, shared_gate, preferred_element_type=jnp.float32)
    up_values = jnp.dot(picked, shared_up, preferred_element_type=jnp.float32)
    hidden = (jax.nn.silu(gate_values) * up_values).astype(jnp.bfloat16)
    shared_part = lax.psum_scatter(
        rounded(jnp.dot(hidden, shared_down, preferred_element_type=jnp.float32)).astype(
            jnp.bfloat16
        ),
        "tp",
        scatter_dimension=0,
        tiled=True,
    ).astype(jnp.float32)
    expert_output = (routed + shared_part).astype(jnp.bfloat16)
    return (mixer_output, expert_output)


def solution(mesh):
    placed = (
        P("ep", None),
        P("ep", None),
        P(),
        P(),
        P(None, "tp"),
        P(None, "tp"),
        P(None, "tp"),
        P("tp"),
        P("tp", None),
        P("ep", None),
        P("ep", None),
        P("ep", None, "tp"),
        P("ep", None, "tp"),
        P("ep", "tp", None),
        P(None, "tp"),
        P(None, "tp"),
        P("tp", None),
    )
    return jax.shard_map(
        local,
        mesh=mesh,
        in_specs=placed,
        out_specs=(P(("ep", "tp"), None), P(("ep", "tp"), None)),
        check_vma=False,
    )
```

profile of v0, /device:TPU:1, one launch (start us, length us, event | category | flops | bytes accessed | tf_op | source)
XLA Modules:
  0.0 414.7 jit_solution(7231487003897511812)
XLA Ops:
  7.2 0.0 copy-start
  7.2 0.0 all-gather.2.cloned.1.call-start
  7.2 0.9 copy.50
  8.2 0.2 reshape.445
  8.4 0.2 eq.28
  8.5 2.1 fusion.3
  10.7 2.4 reduce-window.6
  13.1 0.1 slice.78
  13.2 0.1 copy.52
  13.4 0.2 fusion.38
  13.5 0.5 broadcast.319
  14.0 0.7 fusion.83
  14.7 1.4 scatter_custom_fusion
  16.1 2.1 fusion.5
  18.3 1.4 copy-done.1
  19.7 1.5 concatenate.64
  21.2 7.1 %gather_fusion = bf16[512,2048]{1,0:T(8,128)(2,1)} fusion(bf16[513,2048]{1,0:T(8,128)(2,1)} %concatenate.64, s32[1024]{0:T(1024)S(1)} %pad_clamp_fusion.1), kind=kCustom, calls=%fused_computation | custom fusion | bytes 4196352 | tf_op jit(solution)/shard_map/gather | solution.py:186
  28.3 62.9 %all_to_all.15 = bf16[64,1,8,2048]{3,2,1,0:T(8,128)(2,1)} all-to-all(bf16[64,1,8,2048]{3,2,1,0:T(8,128)(2,1)} %bitcast.203), channel_id=1, replica_groups=mesh['ep'=64,'tp'=4] {'ep'}, dimensions={0} | all-to-all | bytes 4194304 | tf_op jit(solution)/shard_map/all_to_all | solution.py:188
  91.2 0.0 all-gather.2.cloned.1.call-update
  91.2 83.4 %all-gather.2.cloned.1.call-done = bf16[64,4,8,2048]{3,2,1,0:T(8,128)(2,1)} async-done(((bf16[64,1,8,2048]{3,2,1,0:T(8,128)(2,1)}), bf16[64,4,8,2048]{3,2,1,0:T(8,128)(2,1)}) %all-gather.2.cloned.1.call-update) | async-done | bytes 8388624 | tf_op jit(solution)/shard_map/all_gather | solution.py:187
  174.7 7.1 %fusion.27 = f32[64,4,8,256]{3,2,1,0:T(8,128)} fusion(bf16[64,4,8,2048]{3,2,1,0:T(8,128)(2,1)} %all-gather.2.cloned.1.call-done, bf16[1,2048,256]{2,1,0:T(8,128)(2,1)S(1)} %copy-done.10), kind=kOutput, calls=%fused_computation.45 | convolution fusion | flops 2147483648 | bytes 11534336 | tf_op jit(solution)/shard_map/iejcd,edf->iejcf/dot_general | solution.py:197
  181.8 13.7 %convert_bitcast_fusion = bf16[4,64,1,8,2048]{4,3,0,1,2:T(8,128)(2,1)} fusion(bf16[1,256,2048]{2,1,0:T(8,128)(2,1)} %param.30, bf16[64,4,8,2048]{3,2,1,0:T(8,128)(2,1)} %all-gather.2.cloned.1.call-done, f32[64,4,8,256]{3,2,1,0:T(8,128)} %fusion.27, bf16[1,2048,256]{2,1,0:T(8,128)(2,1)} %param.29), kind=kOutput, calls=%fused_computation.3 | convolution fusion | flops 4302307328 | bytes 20971520 | tf_op jit(solution)/shard_map/iejcf,efd->iejcd/dot_general | solution.py:204
  195.5 8.3 %copy.55 = bf16[4,64,1,8,2048]{4,3,1,2,0:T(8,128)(2,1)} copy(bf16[4,64,1,8,2048]{4,3,0,1,2:T(8,128)(2,1)} %convert_bitcast_fusion) | data formatting | bytes 16777216 | tf_op jit(solution)/shard_map/transpose | solution.py:26
  203.8 5.7 %all-to-all-start.1 = ((bf16[4,64,1,8,2048]{4,3,1,2,0:T(8,128)(2,1)}), bf16[4,64,1,8,2048]{4,3,1,2,0:T(8,128)(2,1)}, u32[]{:S(2)}, u32[]{:S(2)}) async-start(bf16[4,64,1,8,2048]{4,3,1,2,0:T(8,128)(2,1)} %copy.55), calls=%async_computation.2 | async-start | bytes 16777216 | tf_op jit(solution)/shard_map/all_to_all | solution.py:31
  209.4 0.0 reduce-scatter.5.cloned.1.call-start
  209.5 2.1 fusion
  211.6 2.6 convolution_convert_fusion.3
  214.3 0.8 fusion.24
  215.1 0.3 fusion.62
  215.5 4.0 collective-permute-start
  219.5 0.7 fusion.85
  220.3 5.3 %convolution_convert_fusion = bf16[512,2048]{1,0:T(8,128)(2,1)} fusion(bf16[128,2048]{1,0:T(8,128)(2,1)S(1)} %copy-done.6, bf16[512,2048]{1,0:T(8,128)(2,1)} %copy-done.1, bf16[2048,128]{1,0:T(8,128)(2,1)S(1)} %copy-done.7, f32[512,128]{1,0:T(8,128)S(1)} %fusion.85), kind=kOutput, calls=%fused_computation.17 | convolution fusion | flops 538312704 | bytes 5505024 | tf_op jit(solution)/shard_map/dot_general | solution.py:220
  225.6 0.0 reduce-scatter.5.cloned.1.call-update
  225.6 3.2 convolution_convert_fusion.2
  228.8 0.1 convert.27
  228.9 0.1 add_compare_fusion
  229.0 0.3 multiply_cosine_fusion
  229.3 0.2 broadcast_and_fusion
  229.5 0.1 fusion.45
  229.7 0.1 copy_bitcast_fusion
  229.9 2.3 fusion.7
  232.2 0.1 broadcast_maximum_fusion
  232.3 87.1 %all-to-all-done.1 = bf16[4,64,1,8,2048]{4,3,1,2,0:T(8,128)(2,1)} async-done(((bf16[4,64,1,8,2048]{4,3,1,2,0:T(8,128)(2,1)}), bf16[4,64,1,8,2048]{4,3,1,2,0:T(8,128)(2,1)}, u32[]{:S(2)}, u32[]{:S(2)}) %all-to-all-start.1) | async-done | bytes 8388640 | tf_op jit(solution)/shard_map/all_to_all | solution.py:31
  319.3 7.3 %reduce_sum.63 = bf16[64,8,2048]{2,1,0:T(8,128)(2,1)} reduce(bf16[4,64,1,8,2048]{4,3,1,2,0:T(8,128)(2,1)} %all-to-all-done.1, bf16[]{:T(256)} %constant.96.clone.1), dimensions={0,2}, to_apply=%region_9.10 | reduce | flops 3145728 | bytes 10485762 | tf_op jit(solution)/shard_map/reduce_sum | solution.py:32
  326.6 11.9 %all-to-all-start.2 = ((bf16[64,1,8,2048]{3,2,1,0:T(8,128)(2,1)}), bf16[64,1,8,2048]{3,2,1,0:T(8,128)(2,1)}, u32[]{:S(2)}, u32[]{:S(2)}) async-start(bf16[64,1,8,2048]{3,2,1,0:T(8,128)(2,1)} %bitcast.204), calls=%async_computation.3 | async-start | bytes 4194304 | tf_op jit(solution)/shard_map/all_to_all | solution.py:208
  338.5 0.3 reduce-scatter.3.cloned.1.call-start
  338.8 2.7 fusion.6
  341.5 0.1 exponential_add_fusion
  341.6 0.0 copy-done.3
  341.6 0.9 fusion.19
  342.6 0.3 copy.49
  342.9 2.6 convolution_convert_fusion.1
  345.5 0.0 reduce-scatter.3.cloned.1.call-update
  345.5 0.7 constant_dynamic-slice_fusion
  346.2 0.1 copy.56
  346.3 0.1 add.207
  346.5 0.1 reshape.469
  346.6 41.4 %all-to-all-done.2 = bf16[64,1,8,2048]{3,2,1,0:T(8,128)(2,1)} async-done(((bf16[64,1,8,2048]{3,2,1,0:T(8,128)(2,1)}), bf16[64,1,8,2048]{3,2,1,0:T(8,128)(2,1)}, u32[]{:S(2)}, u32[]{:S(2)}) %all-to-all-start.2) | async-done | bytes 2097184 | tf_op jit(solution)/shard_map/all_to_all | solution.py:208
  388.1 4.0 bitcast_convert_fusion
  392.1 5.8 %gather_fusion.1 = f32[256,2048]{1,0:T(8,128)} fusion(f32[512,2048]{1,0:T(8,128)} %bitcast_convert_fusion, s32[1024]{0:T(1024)S(1)} %pad_clamp_fusion), kind=kCustom, calls=%fused_computation.1 | custom fusion | bytes 4195328 | tf_op jit(solution)/shard_map/gather | solution.py:213
  397.9 3.5 reshape.468
  401.5 4.7 %multiply_reduce_fusion = f32[128,2048]{1,0:T(8,128)S(1)} fusion(f32[128,2,2048]{2,1,0:T(2,128)} %reshape.468, f32[128,2]{1,0:T(8,128)S(1)} %copy.56), kind=kLoop, calls=%fused_computation.29 | loop fusion | flops 786432 | bytes 3146752 | tf_op jit(solution)/shard_map/reduce_sum | solution.py:214
  406.2 0.0 reduce-scatter.5.cloned.1.call-done
  406.2 1.9 add_convert_fusion
  (54 shorter events, 0.3 us)
Async XLA Ops:
  7.2 335.7 %copy-start = (bf16[384,2048]{1,0:T(8,128)(2,1)S(1)}, bf16[384,2048]{1,0:T(8,128)(2,1)}, u32[]{:S(2)}) copy-start(bf16[384,2048]{1,0:T(8,128)(2,1)} %param.25) | copy-start | bytes 4718596
  7.2 167.5 %all-gather.2.cloned.1.call-start = ((), (), s32[]{:S(2)}) async-start(), calls=%async_computation.6 | async-start | bytes 10485760 | tf_op jit(solution)/shard_map/all_gather | solution.py:187
  8.3 7.8 %copy-start.8 = (f32[2048]{0:T(1024)S(1)}, f32[2048]{0:T(1024)}, u32[]{:S(2)}) copy-start(f32[2048]{0:T(1024)} %param.20) | copy-start | bytes 24580
  18.3 1.4 copy-start.1
  28.3 146.4 %copy-start.10 = (bf16[1,2048,256]{2,1,0:T(8,128)(2,1)S(1)}, bf16[1,2048,256]{2,1,0:T(8,128)(2,1)}, u32[]{:S(2)}) copy-start(bf16[1,2048,256]{2,1,0:T(8,128)(2,1)} %param.28) | copy-start | bytes 3145732
  203.8 115.6 %all-to-all-start.1 = ((bf16[4,64,1,8,2048]{4,3,1,2,0:T(8,128)(2,1)}), bf16[4,64,1,8,2048]{4,3,1,2,0:T(8,128)(2,1)}, u32[]{:S(2)}, u32[]{:S(2)}) async-start(bf16[4,64,1,8,2048]{4,3,1,2,0:T(8,128)(2,1)} %copy.55), calls=%async_computation.2 | async-start | bytes 16777216 | tf_op jit(solution)/shard_map/all_to_all | solution.py:31
  209.4 2.2 copy-start.11
  209.4 2.2 copy-start.13
  209.4 196.8 %reduce-scatter.5.cloned.1.call-start = ((), (), s32[]{:S(2)}) async-start(), calls=%async_computation.7 | async-start | bytes 2621440 | tf_op jit(solution)/shard_map/reduce_scatter | solution.py:219
  211.6 2.7 copy-start.4
  211.6 2.7 copy-start.12
  214.3 5.3 %copy-start.2 = (bf16[512,2048]{1,0:T(8,128)(2,1)S(1)}, bf16[512,2048]{1,0:T(8,128)(2,1)}, u32[]{:S(2)}) copy-start(bf16[512,2048]{1,0:T(8,128)(2,1)} %copy-done.1) | copy-start | bytes 6291460
  214.3 5.3 %copy-start.5 = (bf16[2048,128]{1,0:T(8,128)(2,1)S(1)}, bf16[2048,128]{1,0:T(8,128)(2,1)}, u32[]{:S(2)}) copy-start(bf16[2048,128]{1,0:T(8,128)(2,1)} %param.31) | copy-start | bytes 1572868
  215.1 5.2 %copy-start.6 = (bf16[128,2048]{1,0:T(8,128)(2,1)S(1)}, bf16[128,2048]{1,0:T(8,128)(2,1)}, u32[]{:S(2)}) copy-start(bf16[128,2048]{1,0:T(8,128)(2,1)} %param.33) | copy-start | bytes 1572868
  215.1 5.2 %copy-start.7 = (bf16[2048,128]{1,0:T(8,128)(2,1)S(1)}, bf16[2048,128]{1,0:T(8,128)(2,1)}, u32[]{:S(2)}) copy-start(bf16[2048,128]{1,0:T(8,128)(2,1)} %param.32) | copy-start | bytes 1572868
  215.5 14.3 %collective-permute-start = (bf16[128,128]{0,1:T(8,128)(2,1)S(1)}, bf16[128,128]{0,1:T(8,128)(2,1)S(1)}, u32[]{:S(2)}, u32[]{:S(2)}) collective-permute-start(bf16[128,128]{0,1:T(8,128)(2,1)S(1)} %pad_maximum_fusion.3), channel_id=1, source_target_pairs={{0,4},{4,8},{8,12},{12,16},{16,20},{20,24},{24,28},{28,32},{32,36}... | collective-permute-start | bytes 98312 | tf_op jit(solution)/shard_map/ppermute | solution.py:20
  229.9 2.3 copy-start.9
  326.6 61.5 %all-to-all-start.2 = ((bf16[64,1,8,2048]{3,2,1,0:T(8,128)(2,1)}), bf16[64,1,8,2048]{3,2,1,0:T(8,128)(2,1)}, u32[]{:S(2)}, u32[]{:S(2)}) async-start(bf16[64,1,8,2048]{3,2,1,0:T(8,128)(2,1)} %bitcast.204), calls=%async_computation.3 | async-start | bytes 4194304 | tf_op jit(solution)/shard_map/all_to_all | solution.py:208
  338.5 69.7 %reduce-scatter.3.cloned.1.call-start = ((), (), s32[]{:S(2)}) async-start(), calls=%async_computation.5 | async-start | bytes 2621440 | tf_op jit(solution)/shard_map/reduce_scatter | solution.py:152
  338.8 2.8 copy-start.3
Sparse Core Ops, SparseCore 0:
  91.4 83.2 all-gather.1
  225.7 50.1 reduce-scatter.4
  345.7 31.3 reduce-scatter.2
where the time goes:
time: 416 us; the launch traced here: 415 us
  waiting for transfers between devices  212 us (51%)
  blocking collectives  62.9 us (15%)
  matrix products  39.2 us (9%)
  local copies, waits for them, and re-layouts  32.7 us (8%)
  other arithmetic  31.7 us (8%)
  starting transfers between devices  21.9 us (5%)
  between operations  14.3 us (3%)
    all_to_all x1, waiting for transfers between devices, sent_and_summed(): lax.all_to_all(pieces, axis, split_axis=0, concat_axis=0, tiled=True)  87.1 us
    all_gather x1, waiting for transfers between devices, local(): lax.all_gather(lax.all_to_all(outgoing, 'ep', split_axis=0, concat_axis=0...  83.4 us
    all_to_all x1, blocking collectives, local(): lax.all_to_all(outgoing, 'ep', split_axis=0, concat_axis=0, tiled=True)  62.9 us
    all_to_all x1, waiting for transfers between devices, local(): lax.all_to_all(summed.astype(jnp.bfloat16), 'ep', split_axis=0, concat_ax...  41.4 us
    dot_general x1, matrix products, local(): jnp.einsum('iejcf,efd->iejcd', hidden, expert_down, preferred_element_typ...  13.7 us
    all_to_all x1, starting transfers between devices, local(): lax.all_to_all(summed.astype(jnp.bfloat16), 'ep', split_axis=0, concat_ax...  11.9 us
    gather x2, local copies, waits for them, and re-layouts, local(): gathered = returned[own_slot_index().reshape(own_tokens, top_count)]  9.32 us
  transfers between devices with their start and end apart: 6, of which 3 were waited for; matrix products, arithmetic and copies ran while one was open for 13% of the time, Pallas kernels for 0%

commit v1 on v0

v1 whole, which is shorter than its diff:
```python
import functools
import math

import jax
import jax.numpy as jnp
from jax import lax
from jax.experimental import pallas as pl
from jax.experimental.pallas import tpu as pltpu
from jax.sharding import PartitionSpec as P

HEAD_DIM = 64
WINDOW = 128
MESH = pl.DeviceIdType.MESH

norm_eps = 1e-06
rope_base = 500000.0

GROUP = 512
OWN = 128
WIDTH = 2048
EP = 64
CAP = 8
SLOTS = EP * CAP
PART = 256
SHARED = 128
CHUNKS = 4
COLS = WIDTH // CHUNKS
PAIRS = 3
TP = 4

GATE_L, UP_L, GATE_R, UP_R, GATE_F, UP_F = range(6)
DOWN_L, DOWN_R, DOWN_FL, DOWN_FR = 6, 10, 14, 18
MIX_F, SH_F, MIX_L, SH_L, MIX_R, SH_R, TAIL = range(22, 29)
MESSAGES = 29

f32, bf16 = jnp.float32, jnp.bfloat16


def dot(a, b):
    return jnp.dot(a, b, preferred_element_type=f32)


def kernel(
    xa, xb, wq, wkv, wo, sgate, sup, sdown, gate_in, up_in, down_in,
    gain_a, gain_b, sinks, choice_rows, choice_cols, route, cosine, sine,
    mixer_out, expert_out,
    xa_v, xb_v, na, nb, wq_v, wkv_v, wo_v, sg_v, su_v, sd_v,
    gate, up, down, out, arr, rows, hid, res, ret,
    qs, kvx, att, sh_hid, mix, sh, mix_got, sh_got, routed, weights, picks,
    load_sem, send_sem, recv_sem, x_send, x_recv,
):
    me = lax.axis_index("ep")
    t = lax.axis_index("tp")
    right = lax.rem(t + 1, TP)
    left = lax.rem(t + TP - 1, TP)
    far = lax.rem(t + 2, TP)

    barrier = pltpu.get_barrier_semaphore()

    def greet(s, _):
        pl.semaphore_signal(barrier, inc=1, device_id={"ep": lax.rem(me + s, EP)}, device_id_type=MESH)
        return _

    for neighbour in (left, right):
        pl.semaphore_signal(barrier, inc=1, device_id={"tp": neighbour}, device_id_type=MESH)
    lax.fori_loop(1, EP, greet, 0)

    loads = {}

    def load(name, src, dst):
        copy = pltpu.make_async_copy(src, dst, load_sem.at[len(loads)])
        copy.start()
        loads[name] = copy

    load("xb", xb, xb_v)
    load("sg", sgate, sg_v)
    load("su", sup, su_v)
    load("sd", sdown, sd_v)
    load("xa", xa, xa_v)
    load("wq", wq, wq_v)
    load("wkv", wkv, wkv_v)
    load("wo", wo, wo_v)
    load("gate", gate_in, gate.at[0])
    load("up", up_in, up.at[0])
    for c in range(CHUNKS):
        load(f"down{c}", down_in.at[:, pl.ds(c * COLS, COLS)], down.at[c, pl.ds(0, PART)])

    messages = {}

    def message(number, src, dst, to):
        copy = pltpu.make_async_remote_copy(
            src_ref=src, dst_ref=dst, send_sem=send_sem.at[number], recv_sem=recv_sem.at[number],
            device_id=to, device_id_type=MESH,
        )
        copy.start()
        messages[number] = copy

    own = pl.ds(pl.multiple_of(t * OWN, OWN), OWN)
    row_a = choice_rows[0:1, own].astype(f32)
    row_b = choice_rows[1:2, own].astype(f32)
    cols = choice_cols[own, :].astype(f32)
    col_a, col_b = cols[:, 0:1], cols[:, 1:2]
    down_i = lax.broadcasted_iota(jnp.int32, (OWN, OWN), 0)
    across_i = lax.broadcasted_iota(jnp.int32, (OWN, OWN), 1)

    def count(condition, axis):
        return jnp.sum(jnp.where(condition, 1.0, 0.0).astype(f32), axis=axis, keepdims=True)

    before = down_i < across_i
    after = down_i > across_i
    slot_row_a = row_a * CAP + count((col_a == row_a) & before, 0)
    slot_row_b = row_b * CAP + count(col_a == row_b, 0) + count((col_b == row_b) & before, 0)
    slot_col_a = col_a * CAP + count((col_a == row_a) & after, 1)
    slot_col_b = col_b * CAP + count(col_b == row_a, 1) + count((col_b == row_b) & after, 1)
    slot_i = lax.broadcasted_iota(jnp.int32, (SLOTS, OWN), 0).astype(f32)
    picks[...] = jnp.where((slot_i == slot_row_a) | (slot_i == slot_row_b), 1.0, 0.0).astype(bf16)
    slot_j = lax.broadcasted_iota(jnp.int32, (OWN, SLOTS), 1).astype(f32)
    shares = route[own, :]
    share = jnp.where(slot_j == slot_col_a, shares[:, 0:1], 0.0) + jnp.where(
        slot_j == slot_col_b, shares[:, 1:2], 0.0
    )
    coarse = share.astype(bf16)
    weights[0:OWN, :] = coarse
    weights[OWN:, :] = (share - coarse.astype(f32)).astype(bf16)

    def normalise(src, dst, gain, start, count_of):
        step = 32

        def body(i, _):
            at = pl.ds(pl.multiple_of(start + i * step, step), step)
            wide = src[at, :].astype(f32)
            scale = lax.rsqrt(jnp.mean(wide * wide, axis=-1, keepdims=True) + norm_eps)
            dst[at, :] = (wide * scale * gain[...]).astype(bf16)
            return _

        lax.fori_loop(0, count_of // step, body, 0)

    loads["xb"].wait()
    normalise(xb_v, nb, gain_b, t * OWN, OWN)

    pl.semaphore_wait(barrier, EP + 1)

    message(GATE_L, gate_in, gate.at[1], {"tp": right})
    message(GATE_R, gate_in, gate.at[2], {"tp": left})
    message(UP_L, up_in, up.at[1], {"tp": right})
    message(UP_R, up_in, up.at[2], {"tp": left})

    def gather(c, _):
        at = pl.ds(pl.multiple_of(c * COLS, COLS), COLS)
        got = dot(picks[...], nb[own, at])
        out[:, :, at] = got.reshape(EP, CAP, COLS).astype(bf16)
        return _

    lax.fori_loop(0, CHUNKS, gather, 0)

    def exchange(src_of, dst, number):
        def body(s, _):
            peer = lax.rem(me + s, EP)
            pltpu.make_async_remote_copy(
                src_ref=src_of(peer), dst_ref=dst, send_sem=x_send.at[number], recv_sem=x_recv.at[number],
                device_id={"ep": peer}, device_id_type=MESH,
            ).start()
            return _

        lax.fori_loop(1, EP, body, 0)

    def all_blocks(src, dst, number):
        most = pl.ds(0, EP - 1)
        return pltpu.make_async_remote_copy(
            src_ref=src.at[most], dst_ref=dst.at[most], send_sem=x_send.at[number], recv_sem=x_recv.at[number],
            device_id={"ep": lax.rem(me + 1, EP)}, device_id_type=MESH,
        )

    exchange(lambda peer: out.at[peer], arr.at[me], 0)
    arr[me] = out[me]

    normalise(xb_v, nb, gain_b, 0, GROUP)
    for name in ("sg", "su", "sd"):
        loads[name].wait()

    def shared(i, _):
        at = pl.ds(pl.multiple_of(i * OWN, OWN), OWN)
        g = dot(nb[at, :], sg_v[...])
        u = dot(nb[at, :], su_v[...])
        units = (g / (1.0 + jnp.exp(-g)) * u).astype(bf16)
        for c in range(CHUNKS):
            part = pl.ds(c * COLS, COLS)
            sh[at, part] = dot(units, sd_v[:, part]).astype(bf16)
        return _

    lax.fori_loop(0, TP, shared, 0)

    for name in ("xa", "wq", "wkv"):
        loads[name].wait()
    normalise(xa_v, na, gain_a, 0, GROUP)
    lane = lax.broadcasted_iota(jnp.int32, (OWN, 128), 1)
    first_half = (lane & 63) < 32
    is_key = lane < 64

    def turn(value, c, s):
        value = value.astype(bf16).astype(f32)
        partner = jnp.where(first_half, pltpu.roll(value, 96, 1), pltpu.roll(value, 32, 1))
        return (value * c + partner * s).astype(bf16)

    def project(i, _):
        at = pl.ds(pl.multiple_of(i * OWN, OWN), OWN)
        c, s = cosine[at, :], sine[at, :]
        q = dot(na[at, :], wq_v[...])
        for p in range(PAIRS):
            qs[i, p * OWN : (p + 1) * OWN, :] = turn(q[:, p * 128 : (p + 1) * 128], c, s)
        kv = dot(na[at, :], wkv_v[...])
        after_tail = pl.ds(pl.multiple_of(WINDOW + i * OWN, OWN), OWN)
        kvx[after_tail, :] = turn(kv, jnp.where(is_key, c, 1.0), jnp.where(is_key, s, 0.0))
        return _

    lax.fori_loop(0, TP, project, 0)
    message(TAIL, kvx.at[pl.ds(GROUP, WINDOW)], kvx.at[pl.ds(0, WINDOW)], {"ep": lax.rem(me + 1, EP)})
    messages[TAIL].wait_recv()

    band_lane = lax.broadcasted_iota(jnp.int32, (2 * WINDOW, 128), 1)
    band_key = band_lane < 64
    query_i = lax.broadcasted_iota(jnp.int32, (PAIRS * OWN, 2 * WINDOW), 0) & (WINDOW - 1)
    key_i = lax.broadcasted_iota(jnp.int32, (PAIRS * OWN, 2 * WINDOW), 1)
    distance = query_i + WINDOW - key_i
    in_window = (distance >= 0) & (distance < WINDOW)
    head_row = lax.broadcasted_iota(jnp.int32, (PAIRS * OWN, 1), 0)
    sink_of = [
        jnp.where(
            head_row < OWN, sinks[odd], jnp.where(head_row < 2 * OWN, sinks[2 + odd], sinks[4 + odd])
        )
        for odd in (0, 1)
    ]

    def attend(n, _):
        band = kvx[pl.ds(pl.multiple_of(n * OWN, OWN), 2 * WINDOW), :].astype(f32)
        keys = jnp.where(band_key, band, 0.0)
        values = jnp.where(band_key, 0.0, band)
        key_sets = (keys.astype(bf16), pltpu.roll(keys, 64, 1).astype(bf16))
        value_sets = (pltpu.roll(values, 64, 1).astype(bf16), values.astype(bf16))
        allowed = in_window & (me * GROUP + n * OWN - WINDOW + key_i >= 0)
        q = qs[n]
        total = jnp.zeros((PAIRS * OWN, 128), f32)
        for odd in (0, 1):
            scores = lax.dot_general(
                q, key_sets[odd], (((1,), (1,)), ((), ())), preferred_element_type=f32
            ) * (1.0 / math.sqrt(HEAD_DIM))
            scores = jnp.where(allowed, scores, -jnp.inf)
            peak = jnp.maximum(jnp.max(scores, axis=-1, keepdims=True), sink_of[odd])
            e = jnp.exp(scores - peak)
            denominator = jnp.sum(e, axis=-1, keepdims=True) + jnp.exp(sink_of[odd] - peak)
            total = total + dot((e / denominator).astype(bf16), value_sets[odd])
        at = pl.ds(pl.multiple_of(n * OWN, OWN), OWN)
        for p in range(PAIRS):
            att[at, p * 128 : (p + 1) * 128] = total[p * OWN : (p + 1) * OWN].astype(bf16)
        return _

    lax.fori_loop(0, TP, attend, 0)

    messages[GATE_L].wait_recv()
    message(GATE_F, gate.at[1], gate.at[3], {"tp": right})
    messages[UP_R].wait_recv()
    message(UP_F, up.at[2], up.at[3], {"tp": left})

    def send_down(c):
        src = down_in.at[:, pl.ds(c * COLS, COLS)]
        message(DOWN_L + c, src, down.at[c, pl.ds(PART, PART)], {"tp": right})
        message(DOWN_R + c, src, down.at[c, pl.ds(2 * PART, PART)], {"tp": left})

    send_down(0)
    send_down(1)

    loads["wo"].wait()

    def project_out(i, _):
        at = pl.ds(pl.multiple_of(i * OWN, OWN), OWN)
        for c in range(CHUNKS):
            part = pl.ds(c * COLS, COLS)
            mix[at, part] = dot(att[at, :], wo_v[:, part]).astype(bf16)
        return _

    lax.fori_loop(0, TP, project_out, 0)

    all_blocks(out, arr, 0).wait_recv()

    def flatten(c, _):
        at = pl.ds(pl.multiple_of(c * COLS, COLS), COLS)
        rows[:, at] = arr[:, :, at].astype(f32).reshape(SLOTS, COLS).astype(bf16)
        return _

    lax.fori_loop(0, CHUNKS, flatten, 0)

    def hidden(q):
        def body(i, _):
            at = pl.ds(pl.multiple_of(i * 256, 256), 256)
            g = dot(rows[at, :], gate[q])
            u = dot(rows[at, :], up[q])
            hid[at, q * PART : (q + 1) * PART] = (g / (1.0 + jnp.exp(-g)) * u).astype(bf16)
            return _

        lax.fori_loop(0, SLOTS // 256, body, 0)

    loads["gate"].wait()
    loads["up"].wait()
    hidden(0)
    messages[UP_L].wait_recv()
    hidden(1)
    messages[GATE_R].wait_recv()
    hidden(2)
    messages[GATE_F].wait_recv()
    messages[UP_F].wait_recv()
    hidden(3)

    half = PART // 2

    def finish(c):
        loads[f"down{c}"].wait()
        messages[DOWN_FL + c].wait_recv()
        messages[DOWN_FR + c].wait_recv()

        def body(i, _):
            at = pl.ds(pl.multiple_of(i * 256, 256), 256)
            got = dot(hid[at, :], down[c])
            blocks = pl.ds(i * (256 // CAP), 256 // CAP)
            res[c, blocks] = got.reshape(256 // CAP, CAP, COLS).astype(bf16)
            return _

        lax.fori_loop(0, SLOTS // 256, body, 0)
        exchange(lambda peer: res.at[c, peer], ret.at[c, me], 1 + c)
        ret[c, me] = res[c, me]

    for c in range(CHUNKS):
        messages[DOWN_L + c].wait_recv()
        message(
            DOWN_FL + c, down.at[c, pl.ds(PART, half)], down.at[c, pl.ds(3 * PART, half)], {"tp": right}
        )
        messages[DOWN_R + c].wait_recv()
        message(
            DOWN_FR + c, down.at[c, pl.ds(2 * PART + half, half)], down.at[c, pl.ds(3 * PART + half, half)],
            {"tp": left},
        )
        if c + 2 < CHUNKS:
            send_down(c + 2)
        else:
            if c + 2 == CHUNKS:
                pass
        if c >= 1:
            finish(c - 1)

    def piece(ref, owner):
        return ref.at[pl.ds(pl.multiple_of(owner * OWN, OWN), OWN)]

    message(MIX_F, piece(mix, far), mix_got.at[0], {"tp": right})
    message(SH_F, piece(sh, far), sh_got.at[0], {"tp": left})
    message(SH_L, piece(sh, right), sh_got.at[1], {"tp": right})
    message(MIX_R, piece(mix, left), mix_got.at[2], {"tp": left})
    finish(CHUNKS - 1)

    def combine(c):
        all_blocks(res.at[c], ret.at[c], 1 + c).wait_recv()
        got = ret[c].astype(f32).reshape(SLOTS, COLS).astype(bf16)
        both = dot(weights[...], got)
        routed[:, c * COLS : (c + 1) * COLS] = both[0:OWN] + both[OWN:]

    def add_into(ref, owner, extra):
        at = pl.ds(pl.multiple_of(owner * OWN, OWN), OWN)
        ref[at, :] = (ref[at, :].astype(f32) + extra[...].astype(f32)).astype(bf16)

    combine(0)
    messages[MIX_F].wait_recv()
    add_into(mix, right, mix_got.at[0])
    message(MIX_L, piece(mix, right), mix_got.at[1], {"tp": right})
    messages[SH_F].wait_recv()
    add_into(sh, left, sh_got.at[0])
    message(SH_R, piece(sh, left), sh_got.at[2], {"tp": left})
    for c in range(1, CHUNKS):
        combine(c)

    messages[MIX_R].wait_recv()
    messages[MIX_L].wait_recv()
    mixer_out[...] = (
        mix[own, :].astype(f32) + mix_got[1].astype(f32) + mix_got[2].astype(f32)
    ).astype(bf16)
    messages[SH_L].wait_recv()
    messages[SH_R].wait_recv()
    expert_out[...] = (
        routed[...] + sh[own, :].astype(f32) + sh_got[1].astype(f32) + sh_got[2].astype(f32)
    ).astype(bf16)

    for copy in messages.values():
        copy.wait_send()
    all_blocks(out, arr, 0).wait_send()
    for c in range(CHUNKS):
        all_blocks(res.at[c], ret.at[c], 1 + c).wait_send()


def local(
    mixer_input, expert_input, gain_mixer, gain_expert, query_weight, key_weight, value_weight,
    sink_logits, output_weight, expert_choice, route_weights, expert_gate, expert_up, expert_down,
    shared_gate, shared_up, shared_down,
):
    half_steps = jnp.arange(HEAD_DIM // 2, dtype=f32)
    steps = rope_base ** (-(2.0 * half_steps) / HEAD_DIM)
    positions = (lax.axis_index("ep") * GROUP + jnp.arange(GROUP, dtype=jnp.int32)).astype(f32)
    angles = positions[:, None] * steps[None, :]
    cosine, sine = jnp.cos(angles), jnp.sin(angles)
    cosine = jnp.concatenate([cosine] * 4, axis=1)
    sine = jnp.concatenate([-sine, sine, -sine, sine], axis=1)
    key_value = jnp.concatenate([key_weight, value_weight], axis=1)

    anywhere = pl.BlockSpec(memory_space=pl.ANY)
    vmem = pl.BlockSpec(memory_space=pltpu.VMEM)
    smem = pl.BlockSpec(memory_space=pltpu.SMEM)
    V = pltpu.VMEM
    scratch = [
        V((GROUP, WIDTH), bf16), V((GROUP, WIDTH), bf16), V((GROUP, WIDTH), bf16), V((GROUP, WIDTH), bf16),
        V((WIDTH, 384), bf16), V((WIDTH, 128), bf16), V((384, WIDTH), bf16),
        V((WIDTH, SHARED), bf16), V((WIDTH, SHARED), bf16), V((SHARED, WIDTH), bf16),
        V((TP, WIDTH, PART), bf16), V((TP, WIDTH, PART), bf16), V((CHUNKS, TP * PART, COLS), bf16),
        V((EP, CAP, WIDTH), bf16), V((EP, CAP, WIDTH), bf16), V((SLOTS, WIDTH), bf16),
        V((SLOTS, TP * PART), bf16), V((CHUNKS, EP, CAP, COLS), bf16), V((CHUNKS, EP, CAP, COLS), bf16),
        V((TP, PAIRS * OWN, 128), bf16), V((WINDOW + GROUP, 128), bf16), V((GROUP, 384), bf16),
        V((OWN, SHARED), bf16), V((GROUP, WIDTH), bf16), V((GROUP, WIDTH), bf16),
        V((3, OWN, WIDTH), bf16), V((3, OWN, WIDTH), bf16), V((OWN, WIDTH), f32),
        V((2 * OWN, SLOTS), bf16), V((SLOTS, OWN), bf16),
        pltpu.SemaphoreType.DMA((16,)), pltpu.SemaphoreType.DMA((MESSAGES,)),
        pltpu.SemaphoreType.DMA((MESSAGES,)), pltpu.SemaphoreType.DMA((1 + CHUNKS,)),
        pltpu.SemaphoreType.DMA((1 + CHUNKS,)),
    ]
    shape = jax.ShapeDtypeStruct((OWN, WIDTH), bf16)
    return pl.pallas_call(
        kernel,
        out_shape=(shape, shape),
        in_specs=[anywhere] * 11 + [vmem] * 2 + [smem] + [vmem] * 5,
        out_specs=(vmem, vmem),
        scratch_shapes=scratch,
        compiler_params=pltpu.CompilerParams(
            collective_id=0, has_side_effects=True, vmem_limit_bytes=63 * 2**20
        ),
        name="everything",
    )(
        mixer_input, expert_input, query_weight, key_value, output_weight,
        shared_gate, shared_up, shared_down, expert_gate[0], expert_up[0], expert_down[0],
        gain_mixer[None], gain_expert[None], sink_logits, expert_choice.T, expert_choice, route_weights,
        cosine, sine,
    )


def solution(mesh):
    placed = (
        P("ep", None),
        P("ep", None),
        P(),
        P(),
        P(None, "tp"),
        P(None, "tp"),
        P(None, "tp"),
        P("tp"),
        P("tp", None),
        P("ep", None),
        P("ep", None),
        P("ep", None, "tp"),
        P("ep", None, "tp"),
        P("ep", "tp", None),
        P(None, "tp"),
        P(None, "tp"),
        P("tp", None),
    )
    return jax.shard_map(
        local,
        mesh=mesh,
        in_specs=placed,
        out_specs=(P(("ep", "tp"), None), P(("ep", "tp"), None)),
        check_vma=False,
    )
```

time: 416 us -> 166 us (0.40)
  waiting for transfers between devices: 212 us -> 0 us
  Pallas kernels: 0 us -> 151 us
  blocking collectives: 62.9 us -> 0 us
  matrix products: 39.2 us -> 0 us
  other arithmetic: 31.7 us -> 3.39 us
  local copies, waits for them, and re-layouts: 32.7 us -> 9.29 us
  starting transfers between devices: 21.9 us -> 0 us
  between operations: 14.3 us -> 0.68 us
    pallas_call x0 -> x1, Pallas kernels: none -> 151 us  [local(): pl.pallas_call(kernel, out_shape=(shape, shape), in_specs=[anywhere] * 11...]
    all_to_all x2 -> x0, waiting for transfers between devices: 129 us -> none  [the longest x1 87.1 us: sent_and_summed(): lax.all_to_all(pieces, axis, split_axis=0, concat_axis=0, tiled=True)]
    all_gather x1 -> x0, waiting for transfers between devices: 83.4 us -> none  [local(): lax.all_gather(lax.all_to_all(outgoing, 'ep', split_axis=0, concat_axis=0...]
    all_to_all x1 -> x0, blocking collectives: 62.9 us -> none  [local(): lax.all_to_all(outgoing, 'ep', split_axis=0, concat_axis=0, tiled=True)]
    dot_general x10 -> x0, matrix products: 39.2 us -> none  [the longest x1 13.7 us: local(): jnp.einsum('iejcf,efd->iejcd', hidden, expert_down, preferred_element_typ...]
    reduce_sum x6 -> x0, other arithmetic: 19 us -> none  [the longest x1 7.27 us: sent_and_summed(): return arrived.astype(jnp.float32).sum(axis=0)]
    all_to_all x2 -> x0, starting transfers between devices: 17.5 us -> none  [the longest x1 11.9 us: local(): lax.all_to_all(summed.astype(jnp.bfloat16), 'ep', split_axis=0, concat_ax...]
    gather x3 -> x0, local copies, waits for them, and re-layouts: 16.4 us -> none  [the longest x2 9.32 us: local(): gathered = returned[own_slot_index().reshape(own_tokens, top_count)]]
  transfers between devices with their start and end apart: 6 -> 0, of which waited for: 3 -> 0; matrix products, arithmetic and copies ran while one was open for 13% -> 0% of each run, Pallas kernels for 0% -> 0%
where the time goes in v1:
time: 166 us; the launch traced here: 165 us
  Pallas kernels  151 us (91%)
  local copies, waits for them, and re-layouts  9.29 us (6%)
  other arithmetic  3.39 us (2%)
    pallas_call x1, Pallas kernels, local(): pl.pallas_call(kernel, out_shape=(shape, shape), in_specs=[anywhere] * 11...  151 us
    unnamed x6, local copies, waits for them, and re-layouts  9.29 us

profile of v1, /device:TPU:1, one launch (start us, length us, event | category | flops | bytes accessed | tf_op | source)
XLA Modules:
  0.0 164.6 jit_solution(8474861446089686523)
XLA Ops:
  0.7 1.5 copy.27.route
  2.2 1.5 copy.26.choice_cols
  3.7 1.2 copy.23
  5.0 1.2 copy.24
  6.2 1.1 pad_maximum_fusion.wkv
  7.3 1.0 fusion
  8.3 1.3 pad_maximum_fusion.1
  9.6 151.2 %everything.1 = (bf16[128,2048]{1,0:T(8,128)(2,1)}, bf16[128,2048]{1,0:T(8,128)(2,1)}) custom-call(bf16[512,2048]{1,0:T(8,128)(2,1)} %xa.1, bf16[512,2048]{1,0:T(8,128)(2,1)} %xb.1, bf16[2048,384]{1,0:T(8,128)(2,1)} %wq.1, bf16[2048,128]{1,0:T(8,128)(2,1)} %pad_maximum_fusion.wkv, bf16[384,2048]{1,0:T(8,128)(2,1)} %wo.1, bf16[2048,128]{1,0:T(8,128)(2,1)} %sgate.1, ...), custom_call_target="tpu_custom_call" | custom-call | tf_op jit(solution)/shard_map/everything/pallas_call | solution.py:430
  160.8 1.9 %copy.30 = bf16[128,2048]{1,0:T(8,128)(2,1)} copy(bf16[128,2048]{1,0:T(8,128)(2,1)} %get-tuple-element.9) | data formatting | bytes 1048576
  162.7 1.9 %copy.31 = bf16[128,2048]{1,0:T(8,128)(2,1)} copy(bf16[128,2048]{1,0:T(8,128)(2,1)} %get-tuple-element.10) | data formatting | bytes 1048576
  (2 shorter events, 0.0 us)

commit v2 on v1

v2 whole, which is shorter than its diff:
```python
import functools
import math

import jax
import jax.numpy as jnp
from jax import lax
from jax.experimental import pallas as pl
from jax.experimental.pallas import tpu as pltpu
from jax.sharding import PartitionSpec as P

HEAD_DIM = 64
WINDOW = 128
MESH = pl.DeviceIdType.MESH

norm_eps = 1e-06
rope_base = 500000.0

GROUP = 512
OWN = 128
WIDTH = 2048
EP = 64
CAP = 8
SLOTS = EP * CAP
PART = 256
SHARED = 128
COLS = 512
CUTS = (128, 128, 128, 128) + (256,) * 6
CHUNKS = len(CUTS)
STARTS = tuple(sum(CUTS[:c]) for c in range(CHUNKS))
ROW = 8
STRIP = SHARED // ROW
HALF = WIDTH // 2
PAIRS = 3
TP = 4

GATE_L, UP_L, GATE_R, UP_R, GATE_F, UP_F, TAIL = range(7)
STRIP_L, STRIP_R, STRIP_FL, STRIP_FR, UNITS_L, UNITS_R, UNITS_F = range(7, 14)
MIX_FL, MIX_FR, MIX_L0, MIX_L1, MIX_R0, MIX_R1 = range(14, 20)
DOWN_L, DOWN_R, DOWN_FL, DOWN_FR = (20 + CHUNKS * k for k in range(4))
MESSAGES = 20 + 4 * CHUNKS

f32, bf16 = jnp.float32, jnp.bfloat16


def dot(a, b):
    return jnp.dot(a, b, preferred_element_type=f32)


def kernel(
    xa, xb, wq, wk, wv, wo, sgate, sup, sdown, gate_in, up_in, down_in,
    gain_a_in, gain_b_in, sinks_in, choice_in, route_in, steps_in,
    mixer_out, expert_out,
    xa_v, xb_v, na, nb, wq_v, wkv_v, wo_v, sg_v, su_v, strips,
    gate, up, out, arr, rows, hid,
    gain_a, gain_b, sinks, choice_rows, route, steps,
    qs, kvx, att, mix, mix_far, mix_got, units, units_got, routed, weights, picks,
    *rest,
):
    down, res, ret = (rest[k * CHUNKS : (k + 1) * CHUNKS] for k in range(3))
    load_sem, send_sem, recv_sem, x_send, x_recv = rest[3 * CHUNKS :]
    me = lax.axis_index("ep")
    t = lax.axis_index("tp")
    right = lax.rem(t + 1, TP)
    left = lax.rem(t + TP - 1, TP)
    far = lax.rem(t + 2, TP)

    barrier = pltpu.get_barrier_semaphore()

    def greet(s, _):
        pl.semaphore_signal(barrier, inc=1, device_id={"ep": lax.rem(me + s, EP)}, device_id_type=MESH)
        return _

    for neighbour in (left, right, far):
        pl.semaphore_signal(barrier, inc=1, device_id={"tp": neighbour}, device_id_type=MESH)
    lax.fori_loop(1, EP, greet, 0)

    loads = {}

    def load(name, src, dst):
        copy = pltpu.make_async_copy(src, dst, load_sem.at[len(loads)])
        copy.start()
        loads[name] = copy

    load("choice", choice_in, choice_rows)
    load("route", route_in, route)
    load("gain_b", gain_b_in, gain_b)
    load("xb", xb, xb_v)
    load("gain_a", gain_a_in, gain_a)
    load("sinks", sinks_in, sinks)
    load("steps", steps_in, steps)
    load("sg", sgate, sg_v)
    load("su", sup, su_v)
    load("sd", sdown, strips.at[0])
    load("xa", xa, xa_v)
    load("wq", wq, wq_v)
    load("wk", wk, wkv_v.at[pl.ds(0, HEAD_DIM)])
    load("wv", wv, wkv_v.at[pl.ds(HEAD_DIM, HEAD_DIM)])
    load("wo", wo, wo_v)
    load("gate", gate_in, gate.at[0])
    load("up", up_in, up.at[0])
    for c in range(CHUNKS):
        load(f"down{c}", down_in.at[:, pl.ds(STARTS[c], CUTS[c])], down[c].at[pl.ds(0, PART)])

    messages = {}

    def message(number, src, dst, to):
        copy = pltpu.make_async_remote_copy(
            src_ref=src, dst_ref=dst, send_sem=send_sem.at[number], recv_sem=recv_sem.at[number],
            device_id=to, device_id_type=MESH,
        )
        copy.start()
        messages[number] = copy

    own = pl.ds(pl.multiple_of(t * OWN, OWN), OWN)
    loads["choice"].wait()
    loads["route"].wait()
    row_a = choice_rows[0:1, own].astype(f32)
    row_b = choice_rows[1:2, own].astype(f32)
    down_i = lax.broadcasted_iota(jnp.int32, (OWN, OWN), 0)
    across_i = lax.broadcasted_iota(jnp.int32, (OWN, OWN), 1)

    def column(row):
        return jnp.sum(jnp.where(down_i == across_i, row, 0.0), axis=1, keepdims=True)

    col_a, col_b = column(row_a), column(row_b)

    def count(condition, axis):
        return jnp.sum(jnp.where(condition, 1.0, 0.0).astype(f32), axis=axis, keepdims=True)

    before = down_i < across_i
    after = down_i > across_i
    slot_row_a = row_a * CAP + count((col_a == row_a) & before, 0)
    slot_row_b = row_b * CAP + count(col_a == row_b, 0) + count((col_b == row_b) & before, 0)
    slot_col_a = col_a * CAP + count((col_a == row_a) & after, 1)
    slot_col_b = col_b * CAP + count(col_b == row_a, 1) + count((col_b == row_b) & after, 1)
    slot_i = lax.broadcasted_iota(jnp.int32, (SLOTS, OWN), 0).astype(f32)
    picks[...] = jnp.where((slot_i == slot_row_a) | (slot_i == slot_row_b), 1.0, 0.0).astype(bf16)
    slot_j = lax.broadcasted_iota(jnp.int32, (OWN, SLOTS), 1).astype(f32)
    share = jnp.where(slot_j == slot_col_a, column(route[0:1, own]), 0.0) + jnp.where(
        slot_j == slot_col_b, column(route[1:2, own]), 0.0
    )
    coarse = share.astype(bf16)
    weights[0:OWN, :] = coarse
    weights[OWN:, :] = (share - coarse.astype(f32)).astype(bf16)

    def normalise(src, dst, gain, start, count_of):
        step = 32

        def body(i, _):
            at = pl.ds(pl.multiple_of(start + i * step, step), step)
            wide = src[at, :].astype(f32)
            scale = lax.rsqrt(jnp.mean(wide * wide, axis=-1, keepdims=True) + norm_eps)
            dst[at, :] = (wide * scale * gain[...]).astype(bf16)
            return _

        lax.fori_loop(0, count_of // step, body, 0)

    loads["gain_b"].wait()
    loads["xb"].wait()
    normalise(xb_v, nb, gain_b, t * OWN, OWN)

    pl.semaphore_wait(barrier, EP + 2)

    place = lax.rem(me, ROW)
    strip = pl.ds(pl.multiple_of(place * STRIP, STRIP), STRIP)
    message(STRIP_L, sdown.at[strip], strips.at[1, strip], {"tp": right})
    message(STRIP_R, sdown.at[strip], strips.at[2, strip], {"tp": left})
    message(GATE_L, gate_in, gate.at[1], {"tp": right})
    message(UP_R, up_in, up.at[2], {"tp": left})
    message(UP_L, up_in, up.at[1], {"tp": right})
    message(GATE_R, gate_in, gate.at[2], {"tp": left})

    def send_down(c):
        src = down_in.at[:, pl.ds(STARTS[c], CUTS[c])]
        message(DOWN_L + c, src, down[c].at[pl.ds(PART, PART)], {"tp": right})
        message(DOWN_R + c, src, down[c].at[pl.ds(2 * PART, PART)], {"tp": left})

    send_down(0)

    def gather(c, _):
        at = pl.ds(pl.multiple_of(c * COLS, COLS), COLS)
        got = dot(picks[...], nb[own, at])
        out[:, :, at] = got.reshape(EP, CAP, COLS).astype(bf16)
        return _

    lax.fori_loop(0, WIDTH // COLS, gather, 0)

    def exchange(src_of, dst, number):
        def body(s, _):
            peer = lax.rem(me + s, EP)
            pltpu.make_async_remote_copy(
                src_ref=src_of(peer), dst_ref=dst, send_sem=x_send.at[number], recv_sem=x_recv.at[number],
                device_id={"ep": peer}, device_id_type=MESH,
            ).start()
            return _

        lax.fori_loop(1, EP, body, 0)

    def all_blocks(src, dst, number):
        most = pl.ds(0, EP - 1)
        return pltpu.make_async_remote_copy(
            src_ref=src.at[most], dst_ref=dst.at[most], send_sem=x_send.at[number], recv_sem=x_recv.at[number],
            device_id={"ep": lax.rem(me + 1, EP)}, device_id_type=MESH,
        )

    exchange(lambda peer: out.at[peer], arr.at[me], 0)
    arr[me] = out[me]

    normalise(xb_v, nb, gain_b, 0, GROUP)
    for name in ("sg", "su", "sd"):
        loads[name].wait()

    def shared(i, _):
        at = pl.ds(pl.multiple_of(i * OWN, OWN), OWN)
        g = dot(nb[at, :], sg_v[...])
        u = dot(nb[at, :], su_v[...])
        units[at, :] = (g / (1.0 + jnp.exp(-g)) * u).astype(bf16)
        return _

    lax.fori_loop(0, TP, shared, 0)

    for name in ("xa", "wq", "wk", "wv", "gain_a", "sinks", "steps"):
        loads[name].wait()
    normalise(xa_v, na, gain_a, 0, GROUP)
    lane = lax.broadcasted_iota(jnp.int32, (OWN, 128), 1)
    first_half = (lane & 63) < 32
    is_key = lane < 64

    def turn(value, c, s):
        value = value.astype(bf16).astype(f32)
        partner = jnp.where(first_half, pltpu.roll(value, 96, 1), pltpu.roll(value, 32, 1))
        return (value * c + partner * s).astype(bf16)

    def project(i, _):
        at = pl.ds(pl.multiple_of(i * OWN, OWN), OWN)
        position = me * GROUP + i * OWN + down_i
        angles = position.astype(f32) * steps[...]
        c, s = jnp.cos(angles), jnp.sin(angles)
        s = jnp.where(first_half, -s, s)
        q = dot(na[at, :], wq_v[...])
        for p in range(PAIRS):
            qs[i, p * OWN : (p + 1) * OWN, :] = turn(q[:, p * 128 : (p + 1) * 128], c, s)
        kv = lax.dot_general(na[at, :], wkv_v[...], (((1,), (1,)), ((), ())), preferred_element_type=f32)
        after_tail = pl.ds(pl.multiple_of(WINDOW + i * OWN, OWN), OWN)
        kvx[after_tail, :] = turn(kv, jnp.where(is_key, c, 1.0), jnp.where(is_key, s, 0.0))
        return _

    lax.fori_loop(0, TP, project, 0)
    message(TAIL, kvx.at[pl.ds(GROUP, WINDOW)], kvx.at[pl.ds(0, WINDOW)], {"ep": lax.rem(me + 1, EP)})

    messages[STRIP_L].wait_recv()
    messages[STRIP_R].wait_recv()
    for number, k, part, to in (
        (STRIP_FL, 1, pl.ds(0, HALF), right), (STRIP_FR, 2, pl.ds(HALF, HALF), left),
    ):
        message(number, strips.at[k, strip, part], strips.at[3, strip, part], {"tp": to})

    messages[GATE_L].wait_recv()
    message(GATE_F, gate.at[1], gate.at[3], {"tp": right})
    messages[UP_R].wait_recv()
    message(UP_F, up.at[2], up.at[3], {"tp": left})

    messages[TAIL].wait_recv()

    band_lane = lax.broadcasted_iota(jnp.int32, (2 * WINDOW, 128), 1)
    band_key = band_lane < 64
    query_i = lax.broadcasted_iota(jnp.int32, (PAIRS * OWN, 2 * WINDOW), 0) & (WINDOW - 1)
    key_i = lax.broadcasted_iota(jnp.int32, (PAIRS * OWN, 2 * WINDOW), 1)
    distance = query_i + WINDOW - key_i
    in_window = (distance >= 0) & (distance < WINDOW)
    head_row = lax.broadcasted_iota(jnp.int32, (PAIRS * OWN, 1), 0)

    def sink(head):
        return sinks[0:1, head : head + 1]

    sink_of = [
        jnp.where(
            head_row < OWN, sink(odd), jnp.where(head_row < 2 * OWN, sink(2 + odd), sink(4 + odd))
        )
        for odd in (0, 1)
    ]

    def attend(n, _):
        band = kvx[pl.ds(pl.multiple_of(n * OWN, OWN), 2 * WINDOW), :].astype(f32)
        keys = jnp.where(band_key, band, 0.0)
        values = jnp.where(band_key, 0.0, band)
        key_sets = (keys.astype(bf16), pltpu.roll(keys, 64, 1).astype(bf16))
        value_sets = (pltpu.roll(values, 64, 1).astype(bf16), values.astype(bf16))
        allowed = in_window & (me * GROUP + n * OWN - WINDOW + key_i >= 0)
        q = qs[n]
        total = jnp.zeros((PAIRS * OWN, 128), f32)
        for odd in (0, 1):
            scores = lax.dot_general(
                q, key_sets[odd], (((1,), (1,)), ((), ())), preferred_element_type=f32
            ) * (1.0 / math.sqrt(HEAD_DIM))
            scores = jnp.where(allowed, scores, -jnp.inf)
            peak = jnp.maximum(jnp.max(scores, axis=-1, keepdims=True), sink_of[odd])
            e = jnp.exp(scores - peak)
            denominator = jnp.sum(e, axis=-1, keepdims=True) + jnp.exp(sink_of[odd] - peak)
            total = total + dot((e / denominator).astype(bf16), value_sets[odd])
        at = pl.ds(pl.multiple_of(n * OWN, OWN), OWN)
        for p in range(PAIRS):
            att[at, p * 128 : (p + 1) * 128] = total[p * OWN : (p + 1) * OWN].astype(bf16)
        return _

    lax.fori_loop(0, TP, attend, 0)

    loads["wo"].wait()

    def project_out(i, _):
        at = pl.ds(pl.multiple_of(i * OWN, OWN), OWN)
        for c in range(WIDTH // COLS):
            part = pl.ds(c * COLS, COLS)
            mix[at, part] = dot(att[at, :], wo_v[:, part]).astype(bf16)
        return _

    lax.fori_loop(0, TP, project_out, 0)

    all_blocks(out, arr, 0).wait_recv()

    def flatten(c, _):
        at = pl.ds(pl.multiple_of(c * COLS, COLS), COLS)
        rows[:, at] = arr[:, :, at].astype(f32).reshape(SLOTS, COLS).astype(bf16)
        return _

    lax.fori_loop(0, WIDTH // COLS, flatten, 0)

    def hidden(q):
        def body(i, _):
            at = pl.ds(pl.multiple_of(i * 256, 256), 256)
            g = dot(rows[at, :], gate[q])
            u = dot(rows[at, :], up[q])
            hid[at, q * PART : (q + 1) * PART] = (g / (1.0 + jnp.exp(-g)) * u).astype(bf16)
            return _

        lax.fori_loop(0, SLOTS // 256, body, 0)

    loads["gate"].wait()
    loads["up"].wait()
    hidden(0)
    messages[UP_L].wait_recv()
    hidden(1)
    messages[GATE_R].wait_recv()
    hidden(2)

    foreign = pl.ds(1, TP - 1)
    messages[STRIP_FL].wait_recv()
    messages[STRIP_FR].wait_recv()

    def spread(s, _):
        peer = me - place + lax.rem(place + s, ROW)
        pltpu.make_async_remote_copy(
            src_ref=strips.at[foreign, strip], dst_ref=strips.at[foreign, strip],
            send_sem=x_send.at[1 + CHUNKS], recv_sem=x_recv.at[1 + CHUNKS],
            device_id={"ep": peer}, device_id_type=MESH,
        ).start()
        return _

    lax.fori_loop(1, ROW, spread, 0)
    others = strips.at[foreign, pl.ds(0, SHARED - STRIP)]
    all_strips = pltpu.make_async_remote_copy(
        src_ref=others, dst_ref=others, send_sem=x_send.at[1 + CHUNKS], recv_sem=x_recv.at[1 + CHUNKS],
        device_id={"ep": lax.rem(me + 1, EP)}, device_id_type=MESH,
    )

    half = PART // 2

    def forward_down(c):
        messages[DOWN_L + c].wait_recv()
        message(
            DOWN_FL + c, down[c].at[pl.ds(PART, half)], down[c].at[pl.ds(3 * PART, half)], {"tp": right}
        )
        messages[DOWN_R + c].wait_recv()
        message(
            DOWN_FR + c, down[c].at[pl.ds(2 * PART + half, half)], down[c].at[pl.ds(3 * PART + half, half)],
            {"tp": left},
        )

    forward_down(0)
    send_down(1)
    send_down(2)
    messages[GATE_F].wait_recv()
    messages[UP_F].wait_recv()
    hidden(3)

    def finish(c):
        loads[f"down{c}"].wait()
        messages[DOWN_FL + c].wait_recv()
        messages[DOWN_FR + c].wait_recv()

        def body(i, _):
            at = pl.ds(pl.multiple_of(i * 256, 256), 256)
            got = dot(hid[at, :], down[c][...])
            blocks = pl.ds(i * (256 // CAP), 256 // CAP)
            res[c][blocks] = got.reshape(256 // CAP, CAP, CUTS[c]).astype(bf16)
            return _

        lax.fori_loop(0, SLOTS // 256, body, 0)
        exchange(lambda peer: res[c].at[peer], ret[c].at[me], 1 + c)
        ret[c][me] = res[c][me]

    def piece(ref, owner, columns):
        return ref.at[pl.ds(pl.multiple_of(owner * OWN, OWN), OWN), columns]

    low, high = pl.ds(0, HALF), pl.ds(HALF, HALF)

    finish(0)
    forward_down(1)
    send_down(3)
    for c in range(1, CHUNKS - 1):
        forward_down(c + 1)
        if c + 3 < CHUNKS:
            send_down(c + 3)
        if c + 1 == CHUNKS - 2:
            message(UNITS_L, piece(units, right, pl.ds(0, SHARED)), units_got.at[1], {"tp": right})
            message(UNITS_R, piece(units, left, pl.ds(0, SHARED)), units_got.at[2], {"tp": left})
            message(UNITS_F, piece(units, far, pl.ds(0, SHARED)), units_got.at[3], {"tp": far})
        if c + 1 < CHUNKS - 1:
            finish(c)

    message(MIX_FL, piece(mix, far, low), mix_far.at[0], {"tp": right})
    message(MIX_FR, piece(mix, far, high), mix_far.at[1], {"tp": left})
    message(MIX_L0, piece(mix, right, high), mix_got.at[0, :, high], {"tp": right})
    message(MIX_R0, piece(mix, left, low), mix_got.at[1, :, low], {"tp": left})
    finish(CHUNKS - 2)
    finish(CHUNKS - 1)

    def combine(c):
        all_blocks(res[c], ret[c], 1 + c).wait_recv()
        got = ret[c][...].astype(f32).reshape(SLOTS, CUTS[c]).astype(bf16)
        both = dot(weights[...], got)
        at = pl.ds(STARTS[c], CUTS[c])
        routed[:, at] = routed[:, at] + both[0:OWN] + both[OWN:]

    all_strips.wait_recv()
    for number in (UNITS_L, UNITS_R, UNITS_F):
        messages[number].wait_recv()
    for c in range(WIDTH // COLS):
        at = pl.ds(c * COLS, COLS)
        routed[:, at] = dot(units[own, :], strips[0, :, at]) + sum(
            dot(units_got[k], strips[k, :, at]) for k in range(1, TP)
        )

    def add_into(owner, columns, extra):
        at = pl.ds(pl.multiple_of(owner * OWN, OWN), OWN)
        mix[at, columns] = (mix[at, columns].astype(f32) + extra[...].astype(f32)).astype(bf16)

    combine(0)
    messages[MIX_FL].wait_recv()
    add_into(right, low, mix_far.at[0])
    message(MIX_L1, piece(mix, right, low), mix_got.at[0, :, low], {"tp": right})
    messages[MIX_FR].wait_recv()
    add_into(left, high, mix_far.at[1])
    message(MIX_R1, piece(mix, left, high), mix_got.at[1, :, high], {"tp": left})
    for c in range(1, CHUNKS):
        combine(c)
    expert_out[...] = routed[...].astype(bf16)

    for number in (MIX_L0, MIX_R0, MIX_L1, MIX_R1):
        messages[number].wait_recv()
    mixer_out[...] = (
        mix[own, :].astype(f32) + mix_got[0].astype(f32) + mix_got[1].astype(f32)
    ).astype(bf16)

    for copy in messages.values():
        copy.wait_send()
    all_blocks(out, arr, 0).wait_send()
    for c in range(CHUNKS):
        all_blocks(res[c], ret[c], 1 + c).wait_send()
    all_strips.wait_send()


def hand_on(mixer_in, expert_in, mixer_out, expert_out):
    mixer_out[...] = mixer_in[...]
    expert_out[...] = expert_in[...]


def local(
    mixer_input, expert_input, gain_mixer, gain_expert, query_weight, key_weight, value_weight,
    sink_logits, output_weight, expert_choice, route_weights, expert_gate, expert_up, expert_down,
    shared_gate, shared_up, shared_down,
):
    half_steps = (jnp.arange(128, dtype=jnp.int32) % (HEAD_DIM // 2)).astype(f32)
    steps = (rope_base ** (-(2.0 * half_steps) / HEAD_DIM))[None]
    hbm = pl.BlockSpec(memory_space=pltpu.HBM)
    vmem = pl.BlockSpec(memory_space=pltpu.VMEM)
    V = pltpu.VMEM
    scratch = [
        V((GROUP, WIDTH), bf16), V((GROUP, WIDTH), bf16), V((GROUP, WIDTH), bf16), V((GROUP, WIDTH), bf16),
        V((WIDTH, 384), bf16), V((128, WIDTH), bf16), V((384, WIDTH), bf16),
        V((WIDTH, SHARED), bf16), V((WIDTH, SHARED), bf16), V((TP, SHARED, WIDTH), bf16),
        V((TP, WIDTH, PART), bf16), V((TP, WIDTH, PART), bf16),
        V((EP, CAP, WIDTH), bf16), V((EP, CAP, WIDTH), bf16), V((SLOTS, WIDTH), bf16),
        V((SLOTS, TP * PART), bf16),
        V((1, WIDTH), f32), V((1, WIDTH), f32), V((1, 2 * PAIRS), f32), V((2, GROUP), jnp.int32), V((2, GROUP), f32),
        V((1, 128), f32), V((TP, PAIRS * OWN, 128), bf16), V((WINDOW + GROUP, 128), bf16), V((GROUP, 384), bf16),
        V((GROUP, WIDTH), bf16), V((2, OWN, HALF), bf16), V((2, OWN, WIDTH), bf16),
        V((GROUP, SHARED), bf16), V((TP, OWN, SHARED), bf16), V((OWN, WIDTH), f32),
        V((2 * OWN, SLOTS), bf16), V((SLOTS, OWN), bf16),
        *[V((TP * PART, cut), bf16) for cut in CUTS],
        *[V((EP, CAP, cut), bf16) for cut in CUTS],
        *[V((EP, CAP, cut), bf16) for cut in CUTS],
        pltpu.SemaphoreType.DMA((32,)), pltpu.SemaphoreType.DMA((MESSAGES,)),
        pltpu.SemaphoreType.DMA((MESSAGES,)), pltpu.SemaphoreType.DMA((2 + CHUNKS,)),
        pltpu.SemaphoreType.DMA((2 + CHUNKS,)),
    ]
    shape = jax.ShapeDtypeStruct((OWN, WIDTH), bf16)
    done = pl.pallas_call(
        kernel,
        out_shape=(shape, shape),
        in_specs=[hbm] * 18,
        out_specs=(vmem, vmem),
        scratch_shapes=scratch,
        compiler_params=pltpu.CompilerParams(
            collective_id=0, has_side_effects=True, vmem_limit_bytes=63 * 2**20
        ),
        name="everything",
    )(
        mixer_input, expert_input, query_weight, key_weight.T, value_weight.T, output_weight,
        shared_gate, shared_up, shared_down, expert_gate[0], expert_up[0], expert_down[0],
        gain_mixer[None], gain_expert[None], sink_logits[None], expert_choice.T, route_weights.T, steps,
    )
    return pl.pallas_call(
        hand_on, out_shape=(shape, shape), in_specs=[vmem] * 2, out_specs=(vmem, vmem), name="hand_on"
    )(*done)


def solution(mesh):
    placed = (
        P("ep", None),
        P("ep", None),
        P(),
        P(),
        P(None, "tp"),
        P(None, "tp"),
        P(None, "tp"),
        P("tp"),
        P("tp", None),
        P("ep", None),
        P("ep", None),
        P("ep", None, "tp"),
        P("ep", None, "tp"),
        P("ep", "tp", None),
        P(None, "tp"),
        P(None, "tp"),
        P("tp", None),
    )
    return jax.shard_map(
        local,
        mesh=mesh,
        in_specs=placed,
        out_specs=(P(("ep", "tp"), None), P(("ep", "tp"), None)),
        check_vma=False,
    )
```

time: 166 us -> 144 us (0.87)
  local copies, waits for them, and re-layouts: 9.29 us -> 0 us
  Pallas kernels: 151 us -> 143 us
  other arithmetic: 3.39 us -> 0.52 us
    unnamed x6 -> x0, local copies, waits for them, and re-layouts: 9.29 us -> none
    pallas_call x1 -> x2, Pallas kernels: 151 us -> 143 us  [the longest x1 141 us: local(): pl.pallas_call(kernel, out_shape=(shape, shape), in_specs=[hbm] * 18, out...]
    concatenate x2 -> x0, other arithmetic: 2.39 us -> none  [the longest x1 1.3 us: local(): cosine = jnp.concatenate([cosine] * 4, axis=1)]
where the time goes in v2:
time: 144 us
  Pallas kernels  143 us (99%)
    pallas_call x1, Pallas kernels, local(): pl.pallas_call(kernel, out_shape=(shape, shape), in_specs=[hbm] * 18, out...  141 us

profile of v2, /device:TPU:1, one launch (start us, length us, event | category | flops | bytes accessed | tf_op | source)
XLA Modules:
  0.0 144.1 jit_solution(5847882707836506633)
XLA Ops:
  0.6 0.5 fusion.4.steps_in
  1.2 140.7 %everything.1 = (bf16[128,2048]{1,0:T(8,128)(2,1)}, bf16[128,2048]{1,0:T(8,128)(2,1)}) custom-call(bf16[512,2048]{1,0:T(8,128)(2,1)} %xa.1, bf16[512,2048]{1,0:T(8,128)(2,1)} %xb.1, bf16[2048,384]{1,0:T(8,128)(2,1)} %wq.1, bf16[64,2048]{1,0:T(8,128)(2,1)} %bitcast.13, bf16[64,2048]{1,0:T(8,128)(2,1)} %bitcast.14, bf16[384,2048]{1,0:T(8,128)(2,1)} %wo.1, ...), custom_call_target="tpu_custom_call" | custom-call | tf_op jit(solution)/shard_map/everything/pallas_call | solution.py:508
  141.9 2.2 %hand_on.1 = (bf16[128,2048]{1,0:T(8,128)(2,1)}, bf16[128,2048]{1,0:T(8,128)(2,1)}) custom-call(bf16[128,2048]{1,0:T(8,128)(2,1)} %get-tuple-element.4.mixer_in, bf16[128,2048]{1,0:T(8,128)(2,1)} %get-tuple-element.5.expert_in), custom_call_target="tpu_custom_call" | custom-call | tf_op jit(solution)/shard_map/hand_on/pallas_call | solution.py:523

commit v3 on v2

--- a/solution.py
+++ b/solution.py
@@ -33,11 +33,12 @@
 PAIRS = 3
 TP = 4
 
-GATE_L, UP_L, GATE_R, UP_R, GATE_F, UP_F, TAIL = range(7)
+GATE_L, UP_L, GATE_R, UP_R, TAIL = range(5)
+GATE_F, UP_F = (20 + 4 * CHUNKS, 21 + 4 * CHUNKS), (22 + 4 * CHUNKS, 23 + 4 * CHUNKS)
 STRIP_L, STRIP_R, STRIP_FL, STRIP_FR, UNITS_L, UNITS_R, UNITS_F = range(7, 14)
 MIX_FL, MIX_FR, MIX_L0, MIX_L1, MIX_R0, MIX_R1 = range(14, 20)
 DOWN_L, DOWN_R, DOWN_FL, DOWN_FR = (20 + CHUNKS * k for k in range(4))
-MESSAGES = 20 + 4 * CHUNKS
+MESSAGES = 24 + 4 * CHUNKS
 
 f32, bf16 = jnp.float32, jnp.bfloat16
 
@@ -53,11 +54,11 @@
     xa_v, xb_v, na, nb, wq_v, wkv_v, wo_v, sg_v, su_v, strips,
     gate, up, out, arr, rows, hid,
     gain_a, gain_b, sinks, choice_rows, route, steps,
-    qs, kvx, att, mix, mix_far, mix_got, units, units_got, routed, weights, picks,
+    qs, kvx, att, mix, mix_far, mix_got, units, units_got, routed, weights, picks, mixer_v, expert_v,
     *rest,
 ):
     down, res, ret = (rest[k * CHUNKS : (k + 1) * CHUNKS] for k in range(3))
-    load_sem, send_sem, recv_sem, x_send, x_recv = rest[3 * CHUNKS :]
+    load_sem, send_sem, recv_sem, x_send, x_recv, out_sem = rest[3 * CHUNKS :]
     me = lax.axis_index("ep")
     t = lax.axis_index("tp")
     right = lax.rem(t + 1, TP)
@@ -96,10 +97,6 @@
     load("wk", wk, wkv_v.at[pl.ds(0, HEAD_DIM)])
     load("wv", wv, wkv_v.at[pl.ds(HEAD_DIM, HEAD_DIM)])
     load("wo", wo, wo_v)
-    load("gate", gate_in, gate.at[0])
-    load("up", up_in, up.at[0])
-    for c in range(CHUNKS):
-        load(f"down{c}", down_in.at[:, pl.ds(STARTS[c], CUTS[c])], down[c].at[pl.ds(0, PART)])
 
     messages = {}
 
@@ -110,6 +107,28 @@
         )
         copy.start()
         messages[number] = copy
+
+    pl.semaphore_wait(barrier, EP + 2)
+
+    place = lax.rem(me, ROW)
+    strip = pl.ds(pl.multiple_of(place * STRIP, STRIP), STRIP)
+    message(STRIP_L, sdown.at[strip], strips.at[1, strip], {"tp": right})
+    message(STRIP_R, sdown.at[strip], strips.at[2, strip], {"tp": left})
+    message(GATE_L, gate_in, gate.at[1], {"tp": right})
+    message(UP_R, up_in, up.at[2], {"tp": left})
+    message(UP_L, up_in, up.at[1], {"tp": right})
+    message(GATE_R, gate_in, gate.at[2], {"tp": left})
+
+    def send_down(c):
+        src = down_in.at[:, pl.ds(STARTS[c], CUTS[c])]
+        message(DOWN_L + c, src, down[c].at[pl.ds(PART, PART)], {"tp": right})
+        message(DOWN_R + c, src, down[c].at[pl.ds(2 * PART, PART)], {"tp": left})
+
+    send_down(0)
+    load("gate", gate_in, gate.at[0])
+    load("up", up_in, up.at[0])
+    for c in range(CHUNKS):
+        load(f"down{c}", down_in.at[:, pl.ds(STARTS[c], CUTS[c])], down[c].at[pl.ds(0, PART)])
 
     own = pl.ds(pl.multiple_of(t * OWN, OWN), OWN)
     loads["choice"].wait()
@@ -159,24 +178,6 @@
     loads["xb"].wait()
     normalise(xb_v, nb, gain_b, t * OWN, OWN)
 
-    pl.semaphore_wait(barrier, EP + 2)
-
-    place = lax.rem(me, ROW)
-    strip = pl.ds(pl.multiple_of(place * STRIP, STRIP), STRIP)
-    message(STRIP_L, sdown.at[strip], strips.at[1, strip], {"tp": right})
-    message(STRIP_R, sdown.at[strip], strips.at[2, strip], {"tp": left})
-    message(GATE_L, gate_in, gate.at[1], {"tp": right})
-    message(UP_R, up_in, up.at[2], {"tp": left})
-    message(UP_L, up_in, up.at[1], {"tp": right})
-    message(GATE_R, gate_in, gate.at[2], {"tp": left})
-
-    def send_down(c):
-        src = down_in.at[:, pl.ds(STARTS[c], CUTS[c])]
-        message(DOWN_L + c, src, down[c].at[pl.ds(PART, PART)], {"tp": right})
-        message(DOWN_R + c, src, down[c].at[pl.ds(2 * PART, PART)], {"tp": left})
-
-    send_down(0)
-
     def gather(c, _):
         at = pl.ds(pl.multiple_of(c * COLS, COLS), COLS)
         got = dot(picks[...], nb[own, at])
@@ -256,9 +257,12 @@
         message(number, strips.at[k, strip, part], strips.at[3, strip, part], {"tp": to})
 
     messages[GATE_L].wait_recv()
-    message(GATE_F, gate.at[1], gate.at[3], {"tp": right})
+    halves = [pl.ds(0, PART // 2), pl.ds(PART // 2, PART // 2)]
+    for number, units_at in zip(GATE_F, halves):
+        message(number, gate.at[1, :, units_at], gate.at[3, :, units_at], {"tp": right})
     messages[UP_R].wait_recv()
-    message(UP_F, up.at[2], up.at[3], {"tp": left})
+    for number, units_at in zip(UP_F, halves):
+        message(number, up.at[2, :, units_at], up.at[3, :, units_at], {"tp": left})
 
     messages[TAIL].wait_recv()
 
@@ -325,12 +329,12 @@
 
     lax.fori_loop(0, WIDTH // COLS, flatten, 0)
 
-    def hidden(q):
+    def hidden(q, low_unit=0, high_unit=PART):
         def body(i, _):
             at = pl.ds(pl.multiple_of(i * 256, 256), 256)
-            g = dot(rows[at, :], gate[q])
-            u = dot(rows[at, :], up[q])
-            hid[at, q * PART : (q + 1) * PART] = (g / (1.0 + jnp.exp(-g)) * u).astype(bf16)
+            g = dot(rows[at, :], gate[q, :, low_unit:high_unit])
+            u = dot(rows[at, :], up[q, :, low_unit:high_unit])
+            hid[at, q * PART + low_unit : q * PART + high_unit] = (g / (1.0 + jnp.exp(-g)) * u).astype(bf16)
             return _
 
         lax.fori_loop(0, SLOTS // 256, body, 0)
@@ -379,9 +383,10 @@
     forward_down(0)
     send_down(1)
     send_down(2)
-    messages[GATE_F].wait_recv()
-    messages[UP_F].wait_recv()
-    hidden(3)
+    for k in (0, 1):
+        messages[GATE_F[k]].wait_recv()
+        messages[UP_F[k]].wait_recv()
+        hidden(3, k * (PART // 2), (k + 1) * (PART // 2))
 
     def finish(c):
         loads[f"down{c}"].wait()
@@ -425,12 +430,20 @@
     finish(CHUNKS - 2)
     finish(CHUNKS - 1)
 
+    leaving = []
+
+    def leave(src, dst):
+        copy = pltpu.make_async_copy(src, dst, out_sem.at[len(leaving)])
+        copy.start()
+        leaving.append(copy)
+
     def combine(c):
         all_blocks(res[c], ret[c], 1 + c).wait_recv()
         got = ret[c][...].astype(f32).reshape(SLOTS, CUTS[c]).astype(bf16)
         both = dot(weights[...], got)
         at = pl.ds(STARTS[c], CUTS[c])
-        routed[:, at] = routed[:, at] + both[0:OWN] + both[OWN:]
+        expert_v[:, at] = (routed[:, at] + both[0:OWN] + both[OWN:]).astype(bf16)
+        leave(expert_v.at[:, at], expert_out.at[:, at])
 
     all_strips.wait_recv()
     for number in (UNITS_L, UNITS_R, UNITS_F):
@@ -452,16 +465,19 @@
     messages[MIX_FR].wait_recv()
     add_into(left, high, mix_far.at[1])
     message(MIX_R1, piece(mix, left, high), mix_got.at[1, :, high], {"tp": left})
-    for c in range(1, CHUNKS):
+    for c in range(1, CHUNKS - 1):
         combine(c)
-    expert_out[...] = routed[...].astype(bf16)
 
     for number in (MIX_L0, MIX_R0, MIX_L1, MIX_R1):
         messages[number].wait_recv()
-    mixer_out[...] = (
+    mixer_v[...] = (
         mix[own, :].astype(f32) + mix_got[0].astype(f32) + mix_got[1].astype(f32)
     ).astype(bf16)
-
+    leave(mixer_v, mixer_out)
+    combine(CHUNKS - 1)
+
+    for copy in leaving:
+        copy.wait()
     for copy in messages.values():
         copy.wait_send()
     all_blocks(out, arr, 0).wait_send()
@@ -470,9 +486,20 @@
     all_strips.wait_send()
 
 
-def hand_on(mixer_in, expert_in, mixer_out, expert_out):
-    mixer_out[...] = mixer_in[...]
-    expert_out[...] = expert_in[...]
+def hand_on(mixer_in, expert_in, mixer_out, expert_out, held, in_sem, out_sem):
+    pieces = [(mixer_in, mixer_out, 0), (expert_in, expert_out, 0), (mixer_in, mixer_out, 1), (expert_in, expert_out, 1)]
+    arriving, leaving = [], []
+    for k, (src, _, half) in enumerate(pieces):
+        copy = pltpu.make_async_copy(src.at[pl.ds(half * 64, 64)], held.at[k], in_sem.at[k])
+        copy.start()
+        arriving.append(copy)
+    for k, (_, dst, half) in enumerate(pieces):
+        arriving[k].wait()
+        copy = pltpu.make_async_copy(held.at[k], dst.at[pl.ds(half * 64, 64)], out_sem.at[k])
+        copy.start()
+        leaving.append(copy)
+    for copy in leaving:
+        copy.wait()
 
 
 def local(
@@ -483,7 +510,6 @@
     half_steps = (jnp.arange(128, dtype=jnp.int32) % (HEAD_DIM // 2)).astype(f32)
     steps = (rope_base ** (-(2.0 * half_steps) / HEAD_DIM))[None]
     hbm = pl.BlockSpec(memory_space=pltpu.HBM)
-    vmem = pl.BlockSpec(memory_space=pltpu.VMEM)
     V = pltpu.VMEM
     scratch = [
         V((GROUP, WIDTH), bf16), V((GROUP, WIDTH), bf16), V((GROUP, WIDTH), bf16), V((GROUP, WIDTH), bf16),
@@ -497,19 +523,20 @@
         V((GROUP, WIDTH), bf16), V((2, OWN, HALF), bf16), V((2, OWN, WIDTH), bf16),
         V((GROUP, SHARED), bf16), V((TP, OWN, SHARED), bf16), V((OWN, WIDTH), f32),
         V((2 * OWN, SLOTS), bf16), V((SLOTS, OWN), bf16),
+        V((OWN, WIDTH), bf16), V((OWN, WIDTH), bf16),
         *[V((TP * PART, cut), bf16) for cut in CUTS],
         *[V((EP, CAP, cut), bf16) for cut in CUTS],
         *[V((EP, CAP, cut), bf16) for cut in CUTS],
         pltpu.SemaphoreType.DMA((32,)), pltpu.SemaphoreType.DMA((MESSAGES,)),
         pltpu.SemaphoreType.DMA((MESSAGES,)), pltpu.SemaphoreType.DMA((2 + CHUNKS,)),
-        pltpu.SemaphoreType.DMA((2 + CHUNKS,)),
+        pltpu.SemaphoreType.DMA((2 + CHUNKS,)), pltpu.SemaphoreType.DMA((1 + CHUNKS,)),
     ]
     shape = jax.ShapeDtypeStruct((OWN, WIDTH), bf16)
     done = pl.pallas_call(
         kernel,
         out_shape=(shape, shape),
         in_specs=[hbm] * 18,
-        out_specs=(vmem, vmem),
+        out_specs=(hbm, hbm),
         scratch_shapes=scratch,
         compiler_params=pltpu.CompilerParams(
             collective_id=0, has_side_effects=True, vmem_limit_bytes=63 * 2**20
@@ -521,7 +548,8 @@
         gain_mixer[None], gain_expert[None], sink_logits[None], expert_choice.T, route_weights.T, steps,
     )
     return pl.pallas_call(
-        hand_on, out_shape=(shape, shape), in_specs=[vmem] * 2, out_specs=(vmem, vmem), name="hand_on"
+        hand_on, out_shape=(shape, shape), in_specs=[hbm] * 2, out_specs=(hbm, hbm), name="hand_on",
+        scratch_shapes=[V((4, OWN // 2, WIDTH), bf16), pltpu.SemaphoreType.DMA((4,)), pltpu.SemaphoreType.DMA((4,))],
     )(*done)
 
 

time: 144 us -> 144 us (level)
  no operation moved by 1% of the time
where the time goes in v3:
time: 144 us
  Pallas kernels  143 us (99%)
    pallas_call x1, Pallas kernels, local(): pl.pallas_call(kernel, out_shape=(shape, shape), in_specs=[hbm] * 18, out...  141 us

profile of v3, /device:TPU:1, one launch (start us, length us, event | category | flops | bytes accessed | tf_op | source)
XLA Modules:
  0.0 143.9 jit_solution(16512065515391062995)
XLA Ops:
  0.6 0.5 fusion.4.steps_in
  1.2 140.8 %everything.1 = (bf16[128,2048]{1,0:T(8,128)(2,1)}, bf16[128,2048]{1,0:T(8,128)(2,1)}) custom-call(bf16[512,2048]{1,0:T(8,128)(2,1)} %xa.1, bf16[512,2048]{1,0:T(8,128)(2,1)} %xb.1, bf16[2048,384]{1,0:T(8,128)(2,1)} %wq.1, bf16[64,2048]{1,0:T(8,128)(2,1)} %bitcast.13, bf16[64,2048]{1,0:T(8,128)(2,1)} %bitcast.14, bf16[384,2048]{1,0:T(8,128)(2,1)} %wo.1, ...), custom_call_target="tpu_custom_call" | custom-call | tf_op jit(solution)/shard_map/everything/pallas_call | solution.py:535
  141.9 2.0 %hand_on.1 = (bf16[128,2048]{1,0:T(8,128)(2,1)}, bf16[128,2048]{1,0:T(8,128)(2,1)}) custom-call(bf16[128,2048]{1,0:T(8,128)(2,1)} %get-tuple-element.4.mixer_in, bf16[128,2048]{1,0:T(8,128)(2,1)} %get-tuple-element.5.expert_in), custom_call_target="tpu_custom_call" | custom-call | tf_op jit(solution)/shard_map/hand_on/pallas_call | solution.py:550

commit v4 on v3

--- a/solution.py
+++ b/solution.py
@@ -30,6 +30,7 @@
 ROW = 8
 STRIP = SHARED // ROW
 HALF = WIDTH // 2
+DEPTHS = ((0, 1536), (1536, WIDTH))
 PAIRS = 3
 TP = 4
 
@@ -54,7 +55,7 @@
     xa_v, xb_v, na, nb, wq_v, wkv_v, wo_v, sg_v, su_v, strips,
     gate, up, out, arr, rows, hid,
     gain_a, gain_b, sinks, choice_rows, route, steps,
-    qs, kvx, att, mix, mix_far, mix_got, units, units_got, routed, weights, picks, mixer_v, expert_v,
+    qs, kvx, att, mix, mix_far, mix_got, units, units_got, routed, weights, picks, mixer_v, expert_v, gate_sum, up_sum, first_sum,
     *rest,
 ):
     down, res, ret = (rest[k * CHUNKS : (k + 1) * CHUNKS] for k in range(3))
@@ -257,12 +258,13 @@
         message(number, strips.at[k, strip, part], strips.at[3, strip, part], {"tp": to})
 
     messages[GATE_L].wait_recv()
-    halves = [pl.ds(0, PART // 2), pl.ds(PART // 2, PART // 2)]
-    for number, units_at in zip(GATE_F, halves):
-        message(number, gate.at[1, :, units_at], gate.at[3, :, units_at], {"tp": right})
+    for number, (top, bottom) in zip(GATE_F, DEPTHS):
+        depth = pl.ds(top, bottom - top)
+        message(number, gate.at[1, depth], gate.at[3, depth], {"tp": right})
     messages[UP_R].wait_recv()
-    for number, units_at in zip(UP_F, halves):
-        message(number, up.at[2, :, units_at], up.at[3, :, units_at], {"tp": left})
+    for number, (top, bottom) in zip(UP_F, DEPTHS):
+        depth = pl.ds(top, bottom - top)
+        message(number, up.at[2, depth], up.at[3, depth], {"tp": left})
 
     messages[TAIL].wait_recv()
 
@@ -329,12 +331,18 @@
 
     lax.fori_loop(0, WIDTH // COLS, flatten, 0)
 
-    def hidden(q, low_unit=0, high_unit=PART):
+    def hidden(q, top=0, bottom=WIDTH):
         def body(i, _):
             at = pl.ds(pl.multiple_of(i * 256, 256), 256)
-            g = dot(rows[at, :], gate[q, :, low_unit:high_unit])
-            u = dot(rows[at, :], up[q, :, low_unit:high_unit])
-            hid[at, q * PART + low_unit : q * PART + high_unit] = (g / (1.0 + jnp.exp(-g)) * u).astype(bf16)
+            g = dot(rows[at, top:bottom], gate[q, top:bottom, :])
+            u = dot(rows[at, top:bottom], up[q, top:bottom, :])
+            if top > 0:
+                g, u = g + gate_sum[at, :], u + up_sum[at, :]
+            if bottom < WIDTH:
+                gate_sum[at, :] = g
+                up_sum[at, :] = u
+                return _
+            hid[at, q * PART : (q + 1) * PART] = (g / (1.0 + jnp.exp(-g)) * u).astype(bf16)
             return _
 
         lax.fori_loop(0, SLOTS // 256, body, 0)
@@ -383,19 +391,33 @@
     forward_down(0)
     send_down(1)
     send_down(2)
+
+    near = 3 * PART
+    loads["down0"].wait()
+
+    def begin(i, _):
+        at = pl.ds(pl.multiple_of(i * 256, 256), 256)
+        first_sum[at, :] = dot(hid[at, 0:near], down[0][0:near, :])
+        return _
+
+    lax.fori_loop(0, SLOTS // 256, begin, 0)
     for k in (0, 1):
         messages[GATE_F[k]].wait_recv()
         messages[UP_F[k]].wait_recv()
-        hidden(3, k * (PART // 2), (k + 1) * (PART // 2))
+        hidden(3, *DEPTHS[k])
 
     def finish(c):
-        loads[f"down{c}"].wait()
+        if c > 0:
+            loads[f"down{c}"].wait()
         messages[DOWN_FL + c].wait_recv()
         messages[DOWN_FR + c].wait_recv()
 
         def body(i, _):
             at = pl.ds(pl.multiple_of(i * 256, 256), 256)
-            got = dot(hid[at, :], down[c][...])
+            if c == 0:
+                got = first_sum[at, :] + dot(hid[at, near:], down[0][near:, :])
+            else:
+                got = dot(hid[at, :], down[c][...])
             blocks = pl.ds(i * (256 // CAP), 256 // CAP)
             res[c][blocks] = got.reshape(256 // CAP, CAP, CUTS[c]).astype(bf16)
             return _
@@ -524,6 +546,7 @@
         V((GROUP, SHARED), bf16), V((TP, OWN, SHARED), bf16), V((OWN, WIDTH), f32),
         V((2 * OWN, SLOTS), bf16), V((SLOTS, OWN), bf16),
         V((OWN, WIDTH), bf16), V((OWN, WIDTH), bf16),
+        V((SLOTS, PART), f32), V((SLOTS, PART), f32), V((SLOTS, CUTS[0]), f32),
         *[V((TP * PART, cut), bf16) for cut in CUTS],
         *[V((EP, CAP, cut), bf16) for cut in CUTS],
         *[V((EP, CAP, cut), bf16) for cut in CUTS],

time: 144 us -> 143 us (level)
  no operation moved by 1% of the time
where the time goes in v4:
time: 143 us
  Pallas kernels  142 us (99%)
    pallas_call x1, Pallas kernels, local(): pl.pallas_call(kernel, out_shape=(shape, shape), in_specs=[hbm] * 18, out...  140 us

profile of v4, /device:TPU:1, one launch (start us, length us, event | category | flops | bytes accessed | tf_op | source)
XLA Modules:
  0.0 143.1 jit_solution(8205029212195657680)
XLA Ops:
  0.6 0.5 fusion.4.steps_in
  1.2 139.9 %everything.1 = (bf16[128,2048]{1,0:T(8,128)(2,1)}, bf16[128,2048]{1,0:T(8,128)(2,1)}) custom-call(bf16[512,2048]{1,0:T(8,128)(2,1)} %xa.1, bf16[512,2048]{1,0:T(8,128)(2,1)} %xb.1, bf16[2048,384]{1,0:T(8,128)(2,1)} %wq.1, bf16[64,2048]{1,0:T(8,128)(2,1)} %bitcast.13, bf16[64,2048]{1,0:T(8,128)(2,1)} %bitcast.14, bf16[384,2048]{1,0:T(8,128)(2,1)} %wo.1, ...), custom_call_target="tpu_custom_call" | custom-call | tf_op jit(solution)/shard_map/everything/pallas_call | solution.py:558
  141.1 2.0 %hand_on.1 = (bf16[128,2048]{1,0:T(8,128)(2,1)}, bf16[128,2048]{1,0:T(8,128)(2,1)}) custom-call(bf16[128,2048]{1,0:T(8,128)(2,1)} %get-tuple-element.4.mixer_in, bf16[128,2048]{1,0:T(8,128)(2,1)} %get-tuple-element.5.expert_in), custom_call_target="tpu_custom_call" | custom-call | tf_op jit(solution)/shard_map/hand_on/pallas_call | solution.py:573

commit v5 on v4

--- a/solution.py
+++ b/solution.py
@@ -27,7 +27,7 @@
 CUTS = (128, 128, 128, 128) + (256,) * 6
 CHUNKS = len(CUTS)
 STARTS = tuple(sum(CUTS[:c]) for c in range(CHUNKS))
-ROW = 8
+ROW = 16
 STRIP = SHARED // ROW
 HALF = WIDTH // 2
 DEPTHS = ((0, 1536), (1536, WIDTH))
@@ -52,7 +52,7 @@
     xa, xb, wq, wk, wv, wo, sgate, sup, sdown, gate_in, up_in, down_in,
     gain_a_in, gain_b_in, sinks_in, choice_in, route_in, steps_in,
     mixer_out, expert_out,
-    xa_v, xb_v, na, nb, wq_v, wkv_v, wo_v, sg_v, su_v, strips,
+    xa_v, xb_v, na, nb, wq_v, wkv_v, wo_v, sg_v, su_v, sd_v, strips,
     gate, up, out, arr, rows, hid,
     gain_a, gain_b, sinks, choice_rows, route, steps,
     qs, kvx, att, mix, mix_far, mix_got, units, units_got, routed, weights, picks, mixer_v, expert_v, gate_sum, up_sum, first_sum,
@@ -92,7 +92,7 @@
     load("steps", steps_in, steps)
     load("sg", sgate, sg_v)
     load("su", sup, su_v)
-    load("sd", sdown, strips.at[0])
+    load("sd", sdown, sd_v)
     load("xa", xa, xa_v)
     load("wq", wq, wq_v)
     load("wk", wk, wkv_v.at[pl.ds(0, HEAD_DIM)])
@@ -113,8 +113,8 @@
 
     place = lax.rem(me, ROW)
     strip = pl.ds(pl.multiple_of(place * STRIP, STRIP), STRIP)
-    message(STRIP_L, sdown.at[strip], strips.at[1, strip], {"tp": right})
-    message(STRIP_R, sdown.at[strip], strips.at[2, strip], {"tp": left})
+    message(STRIP_L, sdown.at[strip], strips.at[0, place], {"tp": right})
+    message(STRIP_R, sdown.at[strip], strips.at[1, place], {"tp": left})
     message(GATE_L, gate_in, gate.at[1], {"tp": right})
     message(UP_R, up_in, up.at[2], {"tp": left})
     message(UP_L, up_in, up.at[1], {"tp": right})
@@ -253,9 +253,9 @@
     messages[STRIP_L].wait_recv()
     messages[STRIP_R].wait_recv()
     for number, k, part, to in (
-        (STRIP_FL, 1, pl.ds(0, HALF), right), (STRIP_FR, 2, pl.ds(HALF, HALF), left),
+        (STRIP_FL, 0, pl.ds(0, HALF), right), (STRIP_FR, 1, pl.ds(HALF, HALF), left),
     ):
-        message(number, strips.at[k, strip, part], strips.at[3, strip, part], {"tp": to})
+        message(number, strips.at[k, place, :, part], strips.at[2, place, :, part], {"tp": to})
 
     messages[GATE_L].wait_recv()
     for number, (top, bottom) in zip(GATE_F, DEPTHS):
@@ -355,21 +355,21 @@
     messages[GATE_R].wait_recv()
     hidden(2)
 
-    foreign = pl.ds(1, TP - 1)
+    foreign = pl.ds(0, TP - 1)
     messages[STRIP_FL].wait_recv()
     messages[STRIP_FR].wait_recv()
 
     def spread(s, _):
         peer = me - place + lax.rem(place + s, ROW)
         pltpu.make_async_remote_copy(
-            src_ref=strips.at[foreign, strip], dst_ref=strips.at[foreign, strip],
+            src_ref=strips.at[foreign, place], dst_ref=strips.at[foreign, place],
             send_sem=x_send.at[1 + CHUNKS], recv_sem=x_recv.at[1 + CHUNKS],
             device_id={"ep": peer}, device_id_type=MESH,
         ).start()
         return _
 
     lax.fori_loop(1, ROW, spread, 0)
-    others = strips.at[foreign, pl.ds(0, SHARED - STRIP)]
+    others = strips.at[foreign, pl.ds(0, ROW - 1)]
     all_strips = pltpu.make_async_remote_copy(
         src_ref=others, dst_ref=others, send_sem=x_send.at[1 + CHUNKS], recv_sem=x_recv.at[1 + CHUNKS],
         device_id={"ep": lax.rem(me + 1, EP)}, device_id_type=MESH,
@@ -472,8 +472,9 @@
         messages[number].wait_recv()
     for c in range(WIDTH // COLS):
         at = pl.ds(c * COLS, COLS)
-        routed[:, at] = dot(units[own, :], strips[0, :, at]) + sum(
-            dot(units_got[k], strips[k, :, at]) for k in range(1, TP)
+        routed[:, at] = dot(units[own, :], sd_v[:, at]) + sum(
+            dot(units_got[k], strips[k - 1, :, :, at].astype(f32).reshape(SHARED, COLS).astype(bf16))
+            for k in range(1, TP)
         )
 
     def add_into(owner, columns, extra):
@@ -536,7 +537,7 @@
     scratch = [
         V((GROUP, WIDTH), bf16), V((GROUP, WIDTH), bf16), V((GROUP, WIDTH), bf16), V((GROUP, WIDTH), bf16),
         V((WIDTH, 384), bf16), V((128, WIDTH), bf16), V((384, WIDTH), bf16),
-        V((WIDTH, SHARED), bf16), V((WIDTH, SHARED), bf16), V((TP, SHARED, WIDTH), bf16),
+        V((WIDTH, SHARED), bf16), V((WIDTH, SHARED), bf16), V((SHARED, WIDTH), bf16), V((TP - 1, ROW, STRIP, WIDTH), bf16),
         V((TP, WIDTH, PART), bf16), V((TP, WIDTH, PART), bf16),
         V((EP, CAP, WIDTH), bf16), V((EP, CAP, WIDTH), bf16), V((SLOTS, WIDTH), bf16),
         V((SLOTS, TP * PART), bf16),

time: 143 us -> 143 us (level)
  no operation moved by 1% of the time
where the time goes in v5:
time: 143 us; the launch traced here: 142 us
  Pallas kernels  141 us (99%)
    pallas_call x1, Pallas kernels, local(): pl.pallas_call(kernel, out_shape=(shape, shape), in_specs=[hbm] * 18, out...  139 us

profile of v5, /device:TPU:1, one launch (start us, length us, event | category | flops | bytes accessed | tf_op | source)
XLA Modules:
  0.0 142.5 jit_solution(8170284619875835159)
XLA Ops:
  0.6 0.5 fusion.4.steps_in
  1.2 139.3 %everything.1 = (bf16[128,2048]{1,0:T(8,128)(2,1)}, bf16[128,2048]{1,0:T(8,128)(2,1)}) custom-call(bf16[512,2048]{1,0:T(8,128)(2,1)} %xa.1, bf16[512,2048]{1,0:T(8,128)(2,1)} %xb.1, bf16[2048,384]{1,0:T(8,128)(2,1)} %wq.1, bf16[64,2048]{1,0:T(8,128)(2,1)} %bitcast.13, bf16[64,2048]{1,0:T(8,128)(2,1)} %bitcast.14, bf16[384,2048]{1,0:T(8,128)(2,1)} %wo.1, ...), custom_call_target="tpu_custom_call" | custom-call | tf_op jit(solution)/shard_map/everything/pallas_call | solution.py:559
  140.5 2.0 %hand_on.1 = (bf16[128,2048]{1,0:T(8,128)(2,1)}, bf16[128,2048]{1,0:T(8,128)(2,1)}) custom-call(bf16[128,2048]{1,0:T(8,128)(2,1)} %get-tuple-element.4.mixer_in, bf16[128,2048]{1,0:T(8,128)(2,1)} %get-tuple-element.5.expert_in), custom_call_target="tpu_custom_call" | custom-call | tf_op jit(solution)/shard_map/hand_on/pallas_call | solution.py:574

commit v6 on v5

--- a/solution.py
+++ b/solution.py
@@ -24,13 +24,13 @@
 PART = 256
 SHARED = 128
 COLS = 512
-CUTS = (128, 128, 128, 128) + (256,) * 6
+CUTS = (128, 128, 128, 128) + (256,) * 4 + (512,)
 CHUNKS = len(CUTS)
 STARTS = tuple(sum(CUTS[:c]) for c in range(CHUNKS))
 ROW = 16
 STRIP = SHARED // ROW
 HALF = WIDTH // 2
-DEPTHS = ((0, 1536), (1536, WIDTH))
+DEPTHS = ((0, 1792), (1792, WIDTH))
 PAIRS = 3
 TP = 4
 

time: 143 us -> 141 us (0.986)
  no operation moved by 1% of the time
where the time goes in v6:
time: 141 us
  Pallas kernels  140 us (99%)
    pallas_call x1, Pallas kernels, local(): pl.pallas_call(kernel, out_shape=(shape, shape), in_specs=[hbm] * 18, out...  138 us

profile of v6, /device:TPU:1, one launch (start us, length us, event | category | flops | bytes accessed | tf_op | source)
XLA Modules:
  0.0 141.3 jit_solution(7237554308753331035)
XLA Ops:
  0.6 0.5 fusion.4.steps_in
  1.2 138.1 %everything.1 = (bf16[128,2048]{1,0:T(8,128)(2,1)}, bf16[128,2048]{1,0:T(8,128)(2,1)}) custom-call(bf16[512,2048]{1,0:T(8,128)(2,1)} %xa.1, bf16[512,2048]{1,0:T(8,128)(2,1)} %xb.1, bf16[2048,384]{1,0:T(8,128)(2,1)} %wq.1, bf16[64,2048]{1,0:T(8,128)(2,1)} %bitcast.13, bf16[64,2048]{1,0:T(8,128)(2,1)} %bitcast.14, bf16[384,2048]{1,0:T(8,128)(2,1)} %wo.1, ...), custom_call_target="tpu_custom_call" | custom-call | tf_op jit(solution)/shard_map/everything/pallas_call | solution.py:559
  139.3 2.0 %hand_on.1 = (bf16[128,2048]{1,0:T(8,128)(2,1)}, bf16[128,2048]{1,0:T(8,128)(2,1)}) custom-call(bf16[128,2048]{1,0:T(8,128)(2,1)} %get-tuple-element.4.mixer_in, bf16[128,2048]{1,0:T(8,128)(2,1)} %get-tuple-element.5.expert_in), custom_call_target="tpu_custom_call" | custom-call | tf_op jit(solution)/shard_map/hand_on/pallas_call | solution.py:574
